TPU v7x, 512 devices: a whole 4x8x8 slice. The times are simulated.
512 devices in a mesh: sp: 64 (over z, y), tp: 8 (over x, core).
Axes of the slice: x: 4, y: 8, z: 8, core: 2. Of those that a mesh axis runs over, the one named last changes fastest.
Arguments:
- tokens: bfloat16 [16384, 2048], P('sp', 'tp'), may hold values from -6 to 6
- norm_gain: float32 [2048], replicated, may hold values from 0.1 to 1.9
- query_one: bfloat16 [2048, 512], P(None, 'tp'), may hold values from -6 to 6
- key_one: bfloat16 [2048, 512], P(None, 'tp'), may hold values from -1 to 1
- query_two: bfloat16 [2048, 512], P(None, 'tp'), may hold values from -6 to 6
- key_two: bfloat16 [2048, 512], P(None, 'tp'), may hold values from -1 to 1
- value_weight: bfloat16 [2048, 1024], P(None, 'tp'), may hold values from -0.125 to 0.125
- attn_gate_weight: bfloat16 [2048, 1024], P(None, 'tp'), may hold values from -0.125 to 0.125
- conv_outer: bfloat16 [2048, 1024], P(None, 'tp'), may hold values from -0.125 to 0.125
- conv_inner: bfloat16 [2048, 1024], P(None, 'tp'), may hold values from -0.125 to 0.125
- conv_input: bfloat16 [2048, 1024], P(None, 'tp'), may hold values from -0.125 to 0.125
- conv_taps: bfloat16 [3, 1024], P(None, 'tp'), may hold values from -3.5 to 3.5
- head_lambda: float32 [8], P('tp'), may hold values from 0.3 to 0.8
- head_gain: float32 [128], replicated, may hold values from 0.1 to 1.9
- attn_out_weight: bfloat16 [1024, 2048], P('tp'), may hold values from -0.125 to 0.125
- conv_out_weight: bfloat16 [1024, 2048], P('tp'), may hold values from -0.125 to 0.125
Outputs:
- mixed: bfloat16 [16384, 2048], P(('sp', 'tp'))
All inputs are finite; a program needn't handle non-finite values.
Results may differ from a plain program's by a relative error of at most 0.014.
Values may be sent and summed in bfloat16 or wider, within the bound.
A program may use at most 64 MiB of HBM per device.

v0:
```python
import math

import jax
import jax.numpy as jnp
from jax import lax
from jax.sharding import PartitionSpec as P

D = 2048
KEY_DIM = 64
VALUE_DIM = 128


EPSILON = 1e-06


def in_order(blocks, dim):
    blocks = jnp.moveaxis(blocks, 0, dim)
    shape = blocks.shape
    return blocks.reshape(*shape[:dim], shape[dim] * shape[dim + 1], *shape[dim + 2 :])


def from_everyone(array, axis):
    devices = lax.axis_size(axis)
    return lax.all_to_all(
        jnp.broadcast_to(array[None], (devices, *array.shape)), axis, 0, 0, tiled=True
    )


def gather_directly(array, axis, dim):
    return in_order(from_everyone(array, axis), dim)


def in_one_piece(arrays, axis, dim, along):
    both = jnp.concatenate(arrays, axis=along)
    filled, at, outs = (lax.all_gather(both, axis, axis=dim, tiled=True), 0, [])
    for a in arrays:
        outs.append(lax.slice_in_dim(filled, at, at + a.shape[along], axis=along))
        at += a.shape[along]
    return tuple(outs)


def with_halo(cells, sides, width):
    for axis, dim in sides:
        count = lax.axis_size(axis)
        ends = count - 1
        head = lax.slice_in_dim(cells, 0, width, axis=dim)
        tail = lax.slice_in_dim(cells, cells.shape[dim] - width, cells.shape[dim], axis=dim)
        cells = jnp.concatenate(
            [
                lax.ppermute(tail, axis, [(i, (i + 1) % count) for i in range(ends)]),
                cells,
                lax.ppermute(head, axis, [((i + 1) % count, i) for i in range(ends)]),
            ],
            axis=dim,
        )
    return cells


def in_blocks(array, dim, devices):
    shape = array.shape
    blocks = array.reshape(*shape[:dim], devices, shape[dim] // devices, *shape[dim + 1 :])
    return jnp.moveaxis(blocks, dim, 0)


def sum_at_owner(array, axis, dim):
    devices = lax.axis_size(axis)
    blocks = lax.all_to_all(in_blocks(array, dim, devices), axis, 0, 0, tiled=True)
    return jnp.sum(blocks.astype(jnp.float32), axis=0)


def block_size(length):
    for size in range(min(length, 2048), 0, -1):
        if length % size == 0:
            return size
    return 1


def sweep(states, pieces, handle):
    length = pieces[0].shape[0]
    size = block_size(length)
    count = length // size
    if count == 1:
        return handle(states, pieces)

    def one_turn(index, current):
        subset = tuple((lax.dynamic_slice_in_dim(piece, index * size, size, 0) for piece in pieces))
        return handle(current, subset)

    return lax.fori_loop(0, count, one_turn, states)


def absorb(state, queries, keys, values):
    peak, totals, accum = state
    factor_scale = 1.0 / math.sqrt(queries.shape[2])
    scores = (
        jnp.einsum("qhd,khd->hqk", queries, keys, preferred_element_type=jnp.float32) * factor_scale
    )
    new_peak = jnp.maximum(peak, jnp.max(scores, axis=2, keepdims=True))
    factor = jnp.exp(peak - new_peak)
    weights = jnp.exp(scores - new_peak)
    totals = totals * factor + jnp.sum(weights, axis=2, keepdims=True)
    accum = accum * factor + jnp.einsum(
        "hqk,khe->hqe", weights.astype(jnp.bfloat16), values, preferred_element_type=jnp.float32
    )
    return (new_peak, totals, accum)


def local(
    tokens,
    norm_gain,
    query_one,
    key_one,
    query_two,
    key_two,
    value_weight,
    attn_gate_weight,
    conv_outer,
    conv_inner,
    conv_input,
    conv_taps,
    head_lambda,
    head_gain,
    attn_out_weight,
    conv_out_weight,
):
    row_count = tokens.shape[0]
    heads_here = head_lambda.shape[0]
    matrices = (
        query_one,
        key_one,
        query_two,
        key_two,
        value_weight,
        attn_gate_weight,
        conv_outer,
        conv_inner,
        conv_input,
    )
    stacked = jnp.concatenate(matrices, axis=1)
    widened = gather_directly(tokens, "tp", 1).astype(jnp.float32)
    scaled = (widened * norm_gain).astype(jnp.bfloat16)
    running = jnp.dot(scaled, stacked, preferred_element_type=jnp.float32)
    squares = jnp.sum(widened * widened, axis=1, keepdims=True)
    projected = (running * lax.rsqrt(squares / D + EPSILON)).astype(jnp.bfloat16)
    parts_list = []
    offset = 0
    for matrix in matrices:
        parts_list.append(projected[:, offset : offset + matrix.shape[1]])
        offset = offset + matrix.shape[1]
    first_query, first_key, second_query, second_key, values, attn_gate, outer, inner_a, inner_b = (
        parts_list
    )
    queries_a = first_query.reshape(row_count, heads_here, KEY_DIM)
    queries_b = second_query.reshape(row_count, heads_here, KEY_DIM)
    fresh = (
        jnp.full((heads_here, row_count, 1), -1e30, jnp.float32),
        jnp.zeros((heads_here, row_count, 1), jnp.float32),
        jnp.zeros((heads_here, row_count, VALUE_DIM), jnp.float32),
    )

    def split_keys(keys):
        return keys.reshape(keys.shape[0], heads_here, KEY_DIM)

    def split_values(vals):
        return vals.reshape(vals.shape[0], heads_here, VALUE_DIM)

    def handle_both(states, subset):
        keys_a, keys_b, vals = subset
        shaped = split_values(vals)
        return (
            absorb(states[0], queries_a, split_keys(keys_a), shaped),
            absorb(states[1], queries_b, split_keys(keys_b), shaped),
        )

    state_a, state_b = sweep(
        (fresh, fresh), in_one_piece((first_key, second_key, values), "sp", 0, 1), handle_both
    )
    diff = state_a[2] / state_a[1] - head_lambda[:, None, None] * (state_b[2] / state_b[1])
    normed = diff * lax.rsqrt(jnp.mean(diff * diff, axis=2, keepdims=True) + EPSILON) * head_gain
    normed = normed.transpose(1, 0, 2).reshape(row_count, heads_here * VALUE_DIM)
    attn_mix = (normed * jax.nn.silu(attn_gate.astype(jnp.float32))).astype(jnp.bfloat16)
    product = (inner_a.astype(jnp.float32) * inner_b.astype(jnp.float32)).astype(jnp.bfloat16)
    padded = with_halo(product, (("sp", 0),), 1).astype(jnp.float32)
    taps = conv_taps.astype(jnp.float32)
    convolved = taps[0] * padded[:-2] + taps[1] * padded[1:-1] + taps[2] * padded[2:]
    conv_mix = (outer.astype(jnp.float32) * convolved).astype(jnp.bfloat16)
    summed = sum_at_owner(
        (
            jnp.dot(attn_mix, attn_out_weight, preferred_element_type=jnp.float32)
            + jnp.dot(conv_mix, conv_out_weight, preferred_element_type=jnp.float32)
        ).astype(jnp.bfloat16),
        "tp",
        0,
    )
    return summed.astype(jnp.bfloat16)


def solution(mesh):
    return jax.shard_map(
        local,
        mesh=mesh,
        in_specs=(
            P("sp", "tp"),
            P(),
            P(None, "tp"),
            P(None, "tp"),
            P(None, "tp"),
            P(None, "tp"),
            P(None, "tp"),
            P(None, "tp"),
            P(None, "tp"),
            P(None, "tp"),
            P(None, "tp"),
            P(None, "tp"),
            P("tp"),
            P(),
            P("tp", None),
            P("tp", None),
        ),
        out_specs=P(("sp", "tp"), None),
        check_vma=False,
    )
```

profile of v0, /device:TPU:1, one launch (start us, length us, event | category | flops | bytes accessed | tf_op | source)
XLA Modules:
  0.0 234.4 jit_solution(916844258982814465)
XLA Ops:
  6.5 1.1 copy.23
  7.6 1.1 broadcast_in_dim.51
  8.7 10.4 %all-to-all-start = ((bf16[8,256,256]{1,2,0:T(8,128)(2,1)}), bf16[8,256,256]{1,2,0:T(8,128)(2,1)S(1)}, u32[]{:S(2)}, u32[]{:S(2)}) async-start(bf16[8,256,256]{1,2,0:T(8,128)(2,1)} %broadcast_in_dim.51), calls=%async_computation | async-start | bytes 2097152 | tf_op jit(solution)/shard_map/all_to_all | solution.py:24
  20.0 2.0 copy.27
  22.0 6.6 %concatenate.10 = bf16[2048,896]{1,0:T(8,128)(2,1)} concatenate(bf16[2048,64]{1,0:T(8,128)(2,1)S(1)} %copy.24, bf16[2048,64]{1,0:T(8,128)(2,1)S(1)} %copy.25, bf16[2048,64]{1,0:T(8,128)(2,1)S(1)} %copy.26, bf16[2048,64]{1,0:T(8,128)(2,1)} %copy.27, bf16[2048,128]{1,0:T(8,128)(2,1)} %param.24, bf16[2048,128]{1,0:T(8,128)(2,1)} %param.25, bf16[2048,128]{1,0:T(8,128)(2,1)} %param.26, ...), dimensions={1} | concatenate | bytes 7340032 | tf_op jit(solution)/shard_map/concatenate | solution.py:139
  28.5 5.6 %all-to-all-done = bf16[8,256,256]{1,2,0:T(8,128)(2,1)S(1)} async-done(((bf16[8,256,256]{1,2,0:T(8,128)(2,1)}), bf16[8,256,256]{1,2,0:T(8,128)(2,1)S(1)}, u32[]{:S(2)}, u32[]{:S(2)}) %all-to-all-start) | async-done | bytes 1048608 | tf_op jit(solution)/shard_map/all_to_all | solution.py:24
  34.8 3.3 %fusion.28 = bf16[256,896]{1,0:T(8,128)(2,1)S(1)} fusion(bf16[256,2048]{0,1:T(8,128)(2,1)S(1)} %fusion.27, bf16[2048,896]{1,0:T(8,128)(2,1)} %concatenate.10, f32[256]{0:T(256)S(1)} %add_rsqrt_fusion.1), kind=kOutput, calls=%fused_computation.44 | convolution fusion | flops 939982848 | bytes 5178368 | tf_op jit(solution)/shard_map/dot_general | solution.py:142
  38.3 0.8 pad_maximum_fusion
  39.9 0.6 slice_bitcast_fusion.4
  40.5 1.3 collective-permute-start
  41.8 1.3 collective-permute-start.1
  43.3 2.8 %collective-permute-done.1 = bf16[1,128]{1,0:T(2,128)(2,1)S(1)} collective-permute-done((bf16[1,128]{1,0:T(2,128)(2,1)S(1)}, bf16[1,128]{1,0:T(2,128)(2,1)S(1)}, u32[]{:S(2)}, u32[]{:S(2)}) %collective-permute-start.1) | collective-permute-done | bytes 288 | tf_op jit(solution)/shard_map/ppermute | solution.py:52
  46.1 90.6 %all-gather.2.cloned.1.call-done = bf16[16384,256]{1,0:T(8,128)(2,1)} async-done(((bf16[256,256]{1,0:T(8,128)(2,1)}), bf16[16384,256]{1,0:T(8,128)(2,1)}) %all-gather.2.cloned.1.call-update) | async-done | bytes 8388624 | tf_op jit(solution)/shard_map/all_gather | solution.py:35
  136.7 7.2 %fusion.52 = (bf16[16384,64]{1,0:T(8,128)(2,1)}, bf16[16384,64]{1,0:T(8,128)(2,1)}) fusion(bf16[16384,256]{1,0:T(8,128)(2,1)} %all-gather.2.cloned.1.call-done), kind=kLoop, calls=%fused_computation.83 | loop fusion | bytes 8388608 | tf_op jit(solution)/shard_map/slice | solution.py:37
  143.9 1.5 copy-done.1
  145.4 2.1 slice.82
  147.5 56.7 %while.24 = (s32[]{:T(128)}, f32[1,256,1]{1,2,0:T(1,128)S(1)}, f32[1,256,1]{1,2,0:T(1,128)}, f32[1,256,128]{2,1,0:T(8,128)S(1)}, f32[1,256,1]{1,2,0:T(1,128)S(1)...) while((s32[]{:T(128)}, f32[1,256,1]{1,2,0:T(1,128)S(1)}, ...), condition=%wide.region_6.0_spmd.clone, body=%wide.region_1.0_spmd.clone.sunk | while | flops 409143808 | bytes 15319377 | solution.py:89
  147.5 1.5 fusion.78
  149.4 1.5 fusion.75
  151.0 0.4 fusion.77
  151.4 1.6 fusion.83
  153.0 1.6 fusion.82
  154.6 1.5 fusion.78
  156.5 1.5 fusion.75
  158.1 0.4 fusion.77
  158.5 1.6 fusion.83
  160.1 1.6 fusion.82
  161.7 1.5 fusion.78
  163.6 1.5 fusion.75
  165.2 0.4 fusion.77
  165.6 1.6 fusion.83
  167.2 1.6 fusion.82
  168.8 1.5 fusion.78
  170.3 0.4 fusion.80
  170.7 1.5 fusion.75
  172.3 0.4 fusion.77
  172.7 1.6 fusion.83
  174.3 1.6 fusion.82
  175.9 1.5 fusion.78
  177.8 1.5 fusion.75
  179.4 0.4 fusion.77
  179.8 1.6 fusion.83
  181.3 1.6 fusion.82
  183.0 1.5 fusion.78
  184.9 1.5 fusion.75
  186.4 0.4 fusion.77
  186.9 1.6 fusion.83
  188.4 1.6 fusion.82
  190.1 1.5 fusion.78
  191.6 0.4 fusion.80
  192.0 1.5 fusion.75
  193.5 0.4 fusion.77
  194.0 1.6 fusion.83
  195.5 1.6 fusion.82
  197.2 1.5 fusion.78
  199.1 1.5 fusion.75
  200.6 0.4 fusion.77
  201.0 1.6 fusion.83
  202.6 1.6 fusion.82
  204.3 0.9 multiply_reduce_fusion.1
  205.2 1.1 fusion.38
  206.4 0.4 fusion.26
  206.8 19.9 %all_to_all.10 = bf16[8,32,2048]{2,1,0:T(8,128)(2,1)S(1)} all-to-all(bf16[8,32,2048]{2,1,0:T(8,128)(2,1)S(1)} %bitcast.80), channel_id=1, replica_groups=mesh['sp'=64,'tp'=8] {'tp'}, dimensions={0} | all-to-all | bytes 2097152 | tf_op jit(solution)/shard_map/all_to_all | solution.py:67
  226.8 0.8 reduce_sum.54
  (155 shorter events, 4.6 us)
Async XLA Ops:
  6.5 198.7 %copy-start = (bf16[128,2048]{1,0:T(8,128)(2,1)S(1)}, bf16[128,2048]{1,0:T(8,128)(2,1)}, u32[]{:S(2)}) copy-start(bf16[128,2048]{1,0:T(8,128)(2,1)} %param.32) | copy-start | bytes 1572868
  6.5 12.6 %copy-start.3 = (bf16[2048,64]{0,1:T(8,128)(2,1)S(1)}, bf16[2048,64]{0,1:T(8,128)(2,1)}, u32[]{:S(2)}) copy-start(bf16[2048,64]{0,1:T(8,128)(2,1)} %param.20) | copy-start | bytes 786436
  6.5 12.9 %copy-start.4 = (bf16[2048,64]{0,1:T(8,128)(2,1)S(1)}, bf16[2048,64]{0,1:T(8,128)(2,1)}, u32[]{:S(2)}) copy-start(bf16[2048,64]{0,1:T(8,128)(2,1)} %param.21) | copy-start | bytes 786436
  8.7 11.0 %copy-start.5 = (bf16[2048,64]{0,1:T(8,128)(2,1)S(1)}, bf16[2048,64]{0,1:T(8,128)(2,1)}, u32[]{:S(2)}) copy-start(bf16[2048,64]{0,1:T(8,128)(2,1)} %param.22) | copy-start | bytes 786436
  8.7 25.4 %all-to-all-start = ((bf16[8,256,256]{1,2,0:T(8,128)(2,1)}), bf16[8,256,256]{1,2,0:T(8,128)(2,1)S(1)}, u32[]{:S(2)}, u32[]{:S(2)}) async-start(bf16[8,256,256]{1,2,0:T(8,128)(2,1)} %broadcast_in_dim.51), calls=%async_computation | async-start | bytes 2097152 | tf_op jit(solution)/shard_map/all_to_all | solution.py:24
  19.1 117.6 %all-gather.2.cloned.1.call-start = ((), (), s32[]{:S(2)}) async-start(), calls=%async_computation.2 | async-start | bytes 8519680 | tf_op jit(solution)/shard_map/all_gather | solution.py:35
  22.0 12.5 %copy-start.10 = (f32[2048]{0:T(1024)S(1)}, f32[2048]{0:T(1024)}, u32[]{:S(2)}) copy-start(f32[2048]{0:T(1024)} %param.19) | copy-start | bytes 24580
  34.8 5.0 %copy-start.14 = (bf16[3,128]{1,0:T(4,128)(2,1)S(1)}, bf16[3,128]{1,0:T(4,128)(2,1)}, u32[]{:S(2)}) copy-start(bf16[3,128]{1,0:T(4,128)(2,1)} %param.29) | copy-start | bytes 2308
  40.5 2.8 %collective-permute-start = (bf16[1,128]{1,0:T(2,128)(2,1)S(1)}, bf16[1,128]{1,0:T(2,128)(2,1)S(1)}, u32[]{:S(2)}, u32[]{:S(2)}) collective-permute-start(bf16[1,128]{1,0:T(2,128)(2,1)S(1)} %get-tuple-element.315), channel_id=1, source_target_pairs={{0,8},{8,16},{16,24},{24,32},{32,40},{40,48},{48,56},{56,64},{64,7... | collective-permute-start | bytes 776 | tf_op jit(solution)/shard_map/ppermute | solution.py:50
  41.8 4.3 %collective-permute-start.1 = (bf16[1,128]{1,0:T(2,128)(2,1)S(1)}, bf16[1,128]{1,0:T(2,128)(2,1)S(1)}, u32[]{:S(2)}, u32[]{:S(2)}) collective-permute-start(bf16[1,128]{1,0:T(2,128)(2,1)S(1)} %get-tuple-element.316), channel_id=1, source_target_pairs={{8,0},{16,8},{24,16},{32,24},{40,32},{48,40},{56,48},{64,56},{72,6... | collective-permute-start | bytes 776 | tf_op jit(solution)/shard_map/ppermute | solution.py:52
  136.7 8.8 %copy-start.1 = (bf16[16384,256]{1,0:T(8,128)(2,1)S(1)}, bf16[16384,256]{1,0:T(8,128)(2,1)}, u32[]{:S(2)}) copy-start(bf16[16384,256]{1,0:T(8,128)(2,1)} %all-gather.2.cloned.1.call-done) | copy-start | bytes 25165828
  149.4 1.9 copy-start.6
  149.4 1.9 copy-start.8
  151.4 3.2 %copy-start.7 = (f32[1,256,1]{1,2,0:T(1,128)}, f32[1,256,1]{1,2,0:T(1,128)S(1)}, u32[]{:S(2)}) copy-start(f32[1,256,1]{1,2,0:T(1,128)S(1)} %get-tuple-element.443) | copy-start | bytes 3076 | tf_op jit(solution)/shard_map/while
  151.4 3.2 %copy-start.9 = (f32[1,256,1]{1,2,0:T(1,128)}, f32[1,256,1]{1,2,0:T(1,128)S(1)}, u32[]{:S(2)}) copy-start(f32[1,256,1]{1,2,0:T(1,128)S(1)} %get-tuple-element.446) | copy-start | bytes 3076 | tf_op jit(solution)/shard_map/while
  156.5 1.9 copy-start.6
  156.5 1.9 copy-start.8
  158.5 3.2 %copy-start.7 = (f32[1,256,1]{1,2,0:T(1,128)}, f32[1,256,1]{1,2,0:T(1,128)S(1)}, u32[]{:S(2)}) copy-start(f32[1,256,1]{1,2,0:T(1,128)S(1)} %get-tuple-element.443) | copy-start | bytes 3076 | tf_op jit(solution)/shard_map/while
  158.5 3.2 %copy-start.9 = (f32[1,256,1]{1,2,0:T(1,128)}, f32[1,256,1]{1,2,0:T(1,128)S(1)}, u32[]{:S(2)}) copy-start(f32[1,256,1]{1,2,0:T(1,128)S(1)} %get-tuple-element.446) | copy-start | bytes 3076 | tf_op jit(solution)/shard_map/while
  163.6 1.9 copy-start.6
  163.6 1.9 copy-start.8
  165.6 3.2 %copy-start.7 = (f32[1,256,1]{1,2,0:T(1,128)}, f32[1,256,1]{1,2,0:T(1,128)S(1)}, u32[]{:S(2)}) copy-start(f32[1,256,1]{1,2,0:T(1,128)S(1)} %get-tuple-element.443) | copy-start | bytes 3076 | tf_op jit(solution)/shard_map/while
  165.6 3.2 %copy-start.9 = (f32[1,256,1]{1,2,0:T(1,128)}, f32[1,256,1]{1,2,0:T(1,128)S(1)}, u32[]{:S(2)}) copy-start(f32[1,256,1]{1,2,0:T(1,128)S(1)} %get-tuple-element.446) | copy-start | bytes 3076 | tf_op jit(solution)/shard_map/while
  170.7 1.9 copy-start.6
  170.7 1.9 copy-start.8
  172.7 3.2 %copy-start.7 = (f32[1,256,1]{1,2,0:T(1,128)}, f32[1,256,1]{1,2,0:T(1,128)S(1)}, u32[]{:S(2)}) copy-start(f32[1,256,1]{1,2,0:T(1,128)S(1)} %get-tuple-element.443) | copy-start | bytes 3076 | tf_op jit(solution)/shard_map/while
  172.7 3.2 %copy-start.9 = (f32[1,256,1]{1,2,0:T(1,128)}, f32[1,256,1]{1,2,0:T(1,128)S(1)}, u32[]{:S(2)}) copy-start(f32[1,256,1]{1,2,0:T(1,128)S(1)} %get-tuple-element.446) | copy-start | bytes 3076 | tf_op jit(solution)/shard_map/while
  177.8 1.9 copy-start.6
  177.8 1.9 copy-start.8
  179.8 3.2 %copy-start.7 = (f32[1,256,1]{1,2,0:T(1,128)}, f32[1,256,1]{1,2,0:T(1,128)S(1)}, u32[]{:S(2)}) copy-start(f32[1,256,1]{1,2,0:T(1,128)S(1)} %get-tuple-element.443) | copy-start | bytes 3076 | tf_op jit(solution)/shard_map/while
  179.8 3.2 %copy-start.9 = (f32[1,256,1]{1,2,0:T(1,128)}, f32[1,256,1]{1,2,0:T(1,128)S(1)}, u32[]{:S(2)}) copy-start(f32[1,256,1]{1,2,0:T(1,128)S(1)} %get-tuple-element.446) | copy-start | bytes 3076 | tf_op jit(solution)/shard_map/while
  184.9 1.9 copy-start.6
  184.9 1.9 copy-start.8
  186.8 3.2 %copy-start.7 = (f32[1,256,1]{1,2,0:T(1,128)}, f32[1,256,1]{1,2,0:T(1,128)S(1)}, u32[]{:S(2)}) copy-start(f32[1,256,1]{1,2,0:T(1,128)S(1)} %get-tuple-element.443) | copy-start | bytes 3076 | tf_op jit(solution)/shard_map/while
  186.9 3.2 %copy-start.9 = (f32[1,256,1]{1,2,0:T(1,128)}, f32[1,256,1]{1,2,0:T(1,128)S(1)}, u32[]{:S(2)}) copy-start(f32[1,256,1]{1,2,0:T(1,128)S(1)} %get-tuple-element.446) | copy-start | bytes 3076 | tf_op jit(solution)/shard_map/while
  192.0 1.9 copy-start.6
  192.0 1.9 copy-start.8
  193.9 3.2 %copy-start.7 = (f32[1,256,1]{1,2,0:T(1,128)}, f32[1,256,1]{1,2,0:T(1,128)S(1)}, u32[]{:S(2)}) copy-start(f32[1,256,1]{1,2,0:T(1,128)S(1)} %get-tuple-element.443) | copy-start | bytes 3076 | tf_op jit(solution)/shard_map/while
  193.9 3.2 %copy-start.9 = (f32[1,256,1]{1,2,0:T(1,128)}, f32[1,256,1]{1,2,0:T(1,128)S(1)}, u32[]{:S(2)}) copy-start(f32[1,256,1]{1,2,0:T(1,128)S(1)} %get-tuple-element.446) | copy-start | bytes 3076 | tf_op jit(solution)/shard_map/while
  199.1 1.9 copy-start.6
  199.1 1.9 copy-start.8
  201.0 3.2 %copy-start.7 = (f32[1,256,1]{1,2,0:T(1,128)}, f32[1,256,1]{1,2,0:T(1,128)S(1)}, u32[]{:S(2)}) copy-start(f32[1,256,1]{1,2,0:T(1,128)S(1)} %get-tuple-element.443) | copy-start | bytes 3076 | tf_op jit(solution)/shard_map/while
  201.0 3.2 %copy-start.9 = (f32[1,256,1]{1,2,0:T(1,128)}, f32[1,256,1]{1,2,0:T(1,128)S(1)}, u32[]{:S(2)}) copy-start(f32[1,256,1]{1,2,0:T(1,128)S(1)} %get-tuple-element.446) | copy-start | bytes 3076 | tf_op jit(solution)/shard_map/while
  204.2 2.1 copy-start.2
  204.2 2.1 copy-start.11
  204.3 2.1 copy-start.12
  204.3 2.1 copy-start.13
Sparse Core Ops, SparseCore 0:
  39.3 97.3 all-gather.1
where the time goes:
time: 236 us; the launch traced here: 234 us
  waiting for transfers between devices  99 us (42%)
  matrix products  54.4 us (23%)
  local copies, waits for them, and re-layouts  23.5 us (10%)
  blocking collectives  19.9 us (8%)
  between operations  14.3 us (6%)
  starting transfers between devices  13 us (6%)
  other arithmetic  9.27 us (4%)
    all_gather x1, waiting for transfers between devices, in_one_piece(): filled, at, outs = (lax.all_gather(both, axis, axis=dim, tiled=True), 0, [])  90.6 us
    dot_general x16, matrix products, absorb(): jnp.einsum('hqk,khe->hqe', weights.astype(jnp.bfloat16), values, preferre...  25 us
    dot_general x16, matrix products, absorb(): jnp.einsum('qhd,khd->hqk', queries, keys, preferred_element_type=jnp.floa...  24.5 us
    all_to_all x1, blocking collectives, sum_at_owner(): lax.all_to_all(in_blocks(array, dim, devices), axis, 0, 0, tiled=True)  19.9 us
    all_to_all x1, starting transfers between devices, from_everyone(): lax.all_to_all(jnp.broadcast_to(array[None], (devices, *array.shape)), ax...  10.4 us
    slice x2, local copies, waits for them, and re-layouts, in_one_piece(): outs.append(lax.slice_in_dim(filled, at, at + a.shape[along], axis=along))  9.31 us
    concatenate x1, local copies, waits for them, and re-layouts, local(): stacked = jnp.concatenate(matrices, axis=1)  6.58 us
    reduce_sum x16, other arithmetic, absorb(): totals = totals * factor + jnp.sum(weights, axis=2, keepdims=True)  5.76 us
  transfers between devices with their start and end apart: 4, of which 3 were waited for; matrix products, arithmetic and copies ran while one was open for 4% of the time, Pallas kernels for 0%

commit v1 on v0

v1 whole, which is shorter than its diff:
```python
import math

import jax
import jax.numpy as jnp
from jax import lax
from jax.experimental import pallas as pl
from jax.experimental.pallas import tpu as pltpu
from jax.sharding import PartitionSpec as P

MESH = pl.DeviceIdType.MESH
EPS = 1e-06
BF = jnp.bfloat16
F32 = jnp.float32
T, FB, D, R, KD, VD = 256, 256, 2048, 8, 64, 128
NTP = 8
KEYS = R * T
HALF = D // 2
ROWS = T // NTP
QSCALE = math.log2(math.e) / math.sqrt(KD)


def dot(a, b):
    return jnp.dot(a, b, preferred_element_type=F32)


def kernel(
    tok_h, gain, wq1_h, wk1_h, wq2_h, wk2_h, wv_h, wg_h, wo_h, wi_h, wx_h, taps, lam, hgain, aw_h, cw_h,
    out,
    tok, wn, wall, acc, ss, kb, vb, qb, gate, outer, prod, edge, halo, s1, s2, osend, orecv, tsend, trecv,
    mix, wout, psend, precv,
    lsem, tok_s, tok_r, k_s, k_r, v_s, v_r, q_s, q_r, o_s, o_r, st_s, st_r, h_s, h_r, m_s, m_r, w_s, w_r, p_s, p_r,
):
    sp = lax.axis_index("sp")
    tp = lax.axis_index("tp")
    c = tp % 2
    x = tp // 2
    z = sp // 8
    y = sp % 8
    kpos = (1 - c) * z + c * y
    qpos = (1 - c) * y + c * z
    kstride = 8 - 7 * c
    qstride = 1 + 7 * c
    other = x * 2 + 1 - c

    def kdev(pos):
        return (sp + (pos - kpos) * kstride, tp)

    def qdev(pos):
        return (sp + (pos - qpos) * qstride, tp)

    def remote(src, dst, ssem, rsem, dev):
        return pltpu.make_async_remote_copy(
            src_ref=src, dst_ref=dst, send_sem=ssem, recv_sem=rsem, device_id=dev, device_id_type=MESH
        )

    prev_sp = (sp + 63) % 64
    next_sp = (sp + 1) % 64

    cp_tok = pltpu.make_async_copy(tok_h, tok.at[tp], lsem.at[0])
    cp_tok.start()
    loads = []
    for i, w in enumerate((wq1_h, wq2_h, wk1_h, wk2_h)):
        loads.append(pltpu.make_async_copy(w, wn.at[i], lsem.at[1 + i]))
    for i, w in enumerate((wv_h, wg_h, wo_h, wi_h, wx_h)):
        loads.append(pltpu.make_async_copy(w, wall.at[:, pl.ds(256 + 128 * i, 128)], lsem.at[5 + i]))
    my_half = pl.ds(pl.multiple_of(c * HALF, HALF), HALF)
    other_half = pl.ds(pl.multiple_of((1 - c) * HALF, HALF), HALF)
    loads.append(pltpu.make_async_copy(aw_h.at[:, my_half], wout.at[c, pl.ds(0, VD), :], lsem.at[10]))
    loads.append(pltpu.make_async_copy(cw_h.at[:, my_half], wout.at[c, pl.ds(VD, VD), :], lsem.at[11]))
    for cp in loads:
        cp.start()

    barrier = pltpu.get_barrier_semaphore()

    def greet(dev):
        pl.semaphore_signal(barrier, inc=1, device_id=dev, device_id_type=MESH)

    for d in range(1, 8):
        greet((sp, (tp + d) % 8))
        greet(kdev((kpos + d) % 8))
        greet(qdev((qpos + d) % 8))
    greet((prev_sp, tp))
    greet((next_sp, tp))
    pl.semaphore_wait(barrier, 23)

    cp_tok.wait()

    def tok_to(j):
        return remote(tok.at[tp], tok.at[tp], tok_s.at[j], tok_r.at[tp], (sp, ((x + j) % 4) * 2 + c))

    def tok_fwd(t, slot):
        return remote(tok.at[t], tok.at[t], tok_s.at[slot], tok_r.at[t], (sp, other))

    tok_to(2).start()
    tok_to(1).start()
    tok_to(3).start()
    tok_fwd(tp, 0).start()

    wcopies = [
        remote(aw_h.at[:, other_half], wout.at[c, pl.ds(0, VD), :], w_s.at[0], w_r.at[0], (sp, other)),
        remote(cw_h.at[:, other_half], wout.at[c, pl.ds(VD, VD), :], w_s.at[1], w_r.at[1], (sp, other)),
    ]
    for cp in wcopies:
        cp.start()

    for cp in loads[:4]:
        cp.wait()

    def join(i, carry):
        rows = pl.ds(pl.multiple_of(i * 256, 256), 256)
        wall[rows, pl.ds(0, 128)] = jnp.concatenate([wn[0, rows, :], wn[1, rows, :]], axis=1)
        wall[rows, pl.ds(128, 128)] = jnp.concatenate([wn[2, rows, :], wn[3, rows, :]], axis=1)
        return carry

    lax.fori_loop(0, 8, join, 0)
    for cp in loads[4:9]:
        cp.wait()

    acc[...] = jnp.zeros_like(acc)
    ss[...] = jnp.zeros_like(ss)

    def project(step, carry):
        j = step // 2
        odd = step % 2
        dx = jnp.where(j == 0, 0, jnp.where(j == 1, 3, jnp.where(j == 2, 1, 2)))
        chip = (x + dx) % 4
        cc = (1 - odd) * c + odd * (1 - c)
        t = chip * 2 + cc

        @pl.when(step > 0)
        def _():
            remote(tok.at[t], tok.at[t], tok_s.at[0], tok_r.at[t], (sp, other)).wait_recv()

        @pl.when((step > 1) & (odd == 0))
        def _():
            tok_fwd(t, 3 + j).start()

        block = tok[t].astype(F32)
        sq = block * block
        ss[...] += sq[:, :128] + sq[:, 128:]
        g = gain[:, pl.ds(pl.multiple_of(t * FB, FB), FB)]
        scaled = (block * g).astype(BF)
        acc[...] += dot(scaled, wall[pl.ds(pl.multiple_of(t * FB, FB), FB), :])
        return carry

    lax.fori_loop(0, 8, project, 0)

    inv = lax.rsqrt(jnp.sum(ss[...], axis=1, keepdims=True) / D + EPS)

    kb[kpos] = (acc[:, 128:256] * inv).astype(BF)
    vb[kpos] = (acc[:, 256:384] * inv).T.astype(BF)
    qb[qpos] = (acc[:, 0:128] * (inv * QSCALE)).T.astype(BF)

    def k_to(d):
        return remote(kb.at[kpos], kb.at[kpos], k_s.at[d], k_r.at[kpos], kdev((kpos + d) % 8))

    def v_to(d):
        return remote(vb.at[kpos], vb.at[kpos], v_s.at[d], v_r.at[kpos], kdev((kpos + d) % 8))

    def q_to(d):
        return remote(qb.at[qpos], qb.at[qpos], q_s.at[d], q_r.at[qpos], qdev((qpos + d) % 8))

    order = (4, 3, 5, 2, 6, 1, 7)
    for d in order:
        k_to(d).start()
    for d in order:
        v_to(d).start()
    for d in order:
        q_to(d).start()

    gate[...] = (acc[:, 384:512] * inv).astype(BF)
    outer[...] = (acc[:, 512:640] * inv).astype(BF)
    pr = ((acc[:, 640:768] * inv).astype(BF).astype(F32) * (acc[:, 768:896] * inv).astype(BF).astype(F32)).astype(BF)
    pr = pr.astype(F32)
    prod[...] = pr
    edge[0] = pr[0:8]
    edge[1] = pr[T - 8 : T]
    to_prev = remote(edge.at[0], halo.at[1], h_s.at[0], h_r.at[1], (prev_sp, tp))
    to_next = remote(edge.at[1], halo.at[0], h_s.at[1], h_r.at[0], (next_sp, tp))
    to_prev.start()
    to_next.start()
    to_prev.wait_recv()
    to_next.wait_recv()
    before = jnp.where(sp == 0, 0.0, halo[0][7:8, :])
    after = jnp.where(sp == 63, 0.0, halo[1][0:1, :])
    cur = prod[...]
    rows = lax.broadcasted_iota(jnp.int32, (T, VD), 0)
    up = jnp.where(rows == 0, before, pltpu.roll(cur, 1, 0))
    down = jnp.where(rows == T - 1, after, pltpu.roll(cur, T - 1, 0))
    tp32 = taps[...].astype(F32)
    conv = tp32[0:1] * up + tp32[1:2] * cur + tp32[2:3] * down
    mix[c, :, pl.ds(VD, VD)] = (outer[...].astype(F32) * conv).astype(BF)

    def kv_wait(d, carry):
        pos = (kpos + d) % 8
        remote(kb.at[pos], kb.at[pos], k_s.at[0], k_r.at[pos], kdev(pos)).wait_recv()
        remote(vb.at[pos], vb.at[pos], v_s.at[0], v_r.at[pos], kdev(pos)).wait_recv()
        return carry

    lax.fori_loop(1, 8, kv_wait, 0)

    zero = jnp.zeros((KD, T), BF)

    def scores(qm, n, s_ref, peak):
        s = dot(kb[n], qm)
        s_ref[pl.ds(n * T, T), :] = s
        top = jnp.max(s.reshape(T // 8, 8, T), axis=0)
        return top if peak is None else jnp.maximum(peak, top)

    def apply(n, s_ref, peak, state):
        p = jnp.exp2(s_ref[pl.ds(n * T, T), :] - peak)
        part = jnp.sum(p.reshape(T // 8, 8, T), axis=0)
        o = dot(vb[n], p.astype(BF))
        return (part, o) if state is None else (state[0] + part, state[1] + o)

    def one_block(i, carry):
        odd = i % 2
        mag = 4 - (i + 1) // 2
        off = odd * mag + (1 - odd) * ((8 - mag) % 8)
        pos = (qpos + off) % 8

        @pl.when(i < 7)
        def _():
            remote(qb.at[pos], qb.at[pos], q_s.at[0], q_r.at[pos], qdev(pos)).wait_recv()

        q = qb[pos]
        q1 = jnp.concatenate([q[:KD], zero], axis=0)
        q2 = jnp.concatenate([zero, q[KD:]], axis=0)
        peak = None
        for n in range(R):
            peak = scores(q1, n, s1, peak)
        peak1 = jnp.max(peak, axis=0, keepdims=True)
        peak = None
        state = None
        for n in range(R):
            peak = scores(q2, n, s2, peak)
            state = apply(n, s1, peak1, state)
        peak2 = jnp.max(peak, axis=0, keepdims=True)
        sum1 = jnp.sum(state[0], axis=0, keepdims=True)
        osend[pos, pl.ds(0, VD), :] = state[1].astype(BF)
        state = None
        for n in range(R):
            state = apply(n, s2, peak2, state)
        sum2 = jnp.sum(state[0], axis=0, keepdims=True)
        osend[pos, pl.ds(VD, VD), :] = state[1].astype(BF)
        tsend[pos] = jnp.concatenate([peak1, sum1, peak2, sum2, peak1, sum1, peak2, sum2], axis=0)

        @pl.when(i < 7)
        def _():
            remote(osend.at[pos], orecv.at[qpos], o_s.at[pos], o_r.at[qpos], qdev(pos)).start()
            remote(tsend.at[pos], trecv.at[qpos], st_s.at[pos], st_r.at[qpos], qdev(pos)).start()

        return carry

    lax.fori_loop(0, 8, one_block, 0)

    orecv[qpos] = osend[qpos]
    trecv[qpos] = tsend[qpos]

    def o_wait(d, carry):
        pos = (qpos + d) % 8
        remote(osend.at[pos], orecv.at[pos], o_s.at[pos], o_r.at[pos], qdev(pos)).wait_recv()
        remote(tsend.at[pos], trecv.at[pos], st_s.at[pos], st_r.at[pos], qdev(pos)).wait_recv()
        return carry

    lax.fori_loop(1, 8, o_wait, 0)

    def merged(row, at):
        peak = trecv[0, pl.ds(row, 1), :]
        for n in range(1, R):
            peak = jnp.maximum(peak, trecv[n, pl.ds(row, 1), :])
        total = None
        for n in range(R):
            w = jnp.exp2(trecv[n, pl.ds(row, 1), :] - peak)
            part = w * trecv[n, pl.ds(row + 1, 1), :]
            o = w * orecv[n, pl.ds(at, VD), :].astype(F32)
            total = (part, o) if total is None else (total[0] + part, total[1] + o)
        return total[1] / total[0]

    diff = merged(0, 0) - lam[0] * merged(2, VD)
    diff = (diff * lax.rsqrt(jnp.mean(diff * diff, axis=0, keepdims=True) + EPS)).T
    g32 = gate[...].astype(F32)
    mix[c, :, pl.ds(0, VD)] = (diff * hgain[...] * (g32 / (1.0 + jnp.exp(-g32)))).astype(BF)

    share = remote(mix.at[c], mix.at[c], m_s, m_r, (sp, other))
    share.start()
    for cp in loads[9:]:
        cp.wait()
    for i in range(2):
        wcopies[i].wait_recv()
    share.wait_recv()

    def p_copy(chip, core):
        return remote(
            psend.at[chip, pl.ds(pl.multiple_of(core * ROWS, ROWS), ROWS), :],
            precv.at[tp],
            p_s.at[chip * 2 + core],
            p_r.at[tp],
            (sp, chip * 2 + core),
        )

    def to_chip(i, carry):
        chip = (x + jnp.where(i == 0, 2, jnp.where(i == 1, 1, jnp.where(i == 2, 3, 0)))) % 4
        rows = pl.ds(pl.multiple_of(chip * 2 * ROWS, 2 * ROWS), 2 * ROWS)
        psend[chip] = (dot(mix[0, rows, :], wout[0]) + dot(mix[1, rows, :], wout[1])).astype(BF)

        @pl.when(i < 3)
        def _():
            p_copy(chip, c).start()

        p_copy(chip, 1 - c).start()
        return carry

    lax.fori_loop(0, 4, to_chip, 0)
    precv[tp] = psend[x, pl.ds(pl.multiple_of(c * ROWS, ROWS), ROWS), :]

    def p_wait(d, carry):
        src = (tp + d) % 8
        remote(
            psend.at[0, pl.ds(0, ROWS), :], precv.at[src], p_s.at[0], p_r.at[src], (sp, src)
        ).wait_recv()
        return carry

    lax.fori_loop(1, 8, p_wait, 0)
    for half in range(2):
        total = precv[half].astype(F32)
        for n in range(1, 4):
            total += precv[2 * n + half].astype(F32)
        out[:, pl.ds(half * HALF, HALF)] = total.astype(BF)

    tok_fwd(tp, 0).wait_send()
    for j in (1, 2, 3):
        tok_to(j).wait_send()
        tok_fwd(tp, 3 + j).wait_send()
    for d in range(1, 8):
        k_to(d).wait_send()
        v_to(d).wait_send()
        q_to(d).wait_send()
        pos = (qpos + d) % 8
        remote(osend.at[pos], orecv.at[qpos], o_s.at[pos], o_r.at[qpos], qdev(pos)).wait_send()
        remote(tsend.at[pos], trecv.at[qpos], st_s.at[pos], st_r.at[qpos], qdev(pos)).wait_send()
        dst = (tp + d) % 8
        p_copy(dst // 2, dst % 2).wait_send()
    to_prev.wait_send()
    to_next.wait_send()
    share.wait_send()
    for cp in wcopies:
        cp.wait_send()


def local(tokens, norm_gain, q1, k1, q2, k2, wv, wg, wo, wi, wx, taps, lam, hgain, aw, cw):
    hbm = pl.BlockSpec(memory_space=pl.ANY)
    vm = pl.BlockSpec(memory_space=pltpu.VMEM)
    sm = pl.BlockSpec(memory_space=pltpu.SMEM)
    dma = pltpu.SemaphoreType.DMA
    v = pltpu.VMEM
    return pl.pallas_call(
        kernel,
        out_shape=jax.ShapeDtypeStruct((ROWS, D), BF),
        in_specs=[hbm, vm] + [hbm] * 9 + [vm, sm, vm, hbm, hbm],
        out_specs=vm,
        scratch_shapes=[
            v((8, T, FB), BF), v((4, D, KD), BF), v((D, 896), BF), v((T, 896), F32), v((T, 128), F32),
            v((R, T, 128), BF), v((R, VD, T), BF), v((R, 128, T), BF),
            v((T, VD), BF), v((T, VD), BF), v((T, VD), F32), v((2, 8, VD), F32), v((2, 8, VD), F32),
            v((KEYS, T), F32), v((KEYS, T), F32),
            v((R, 2 * VD, T), BF), v((R, 2 * VD, T), BF), v((R, 8, T), F32), v((R, 8, T), F32),
            v((2, T, 2 * VD), BF), v((2, 2 * VD, HALF), BF), v((4, 2 * ROWS, HALF), BF), v((8, ROWS, HALF), BF),
            dma((12,)), dma((8,)), dma((8,)), dma((8,)), dma((8,)), dma((8,)), dma((8,)), dma((8,)), dma((8,)),
            dma((8,)), dma((8,)), dma((8,)), dma((8,)), dma((2,)), dma((2,)), dma, dma, dma((2,)), dma((2,)),
            dma((8,)), dma((8,)),
        ],
        compiler_params=pltpu.CompilerParams(
            collective_id=0, has_side_effects=True, vmem_limit_bytes=48 * 1024 * 1024
        ),
        name="layer",
    )(tokens, norm_gain.reshape(1, D), q1, k1, q2, k2, wv, wg, wo, wi, wx, taps, lam, hgain.reshape(1, VD), aw, cw)


def solution(mesh):
    col = P(None, "tp")
    return jax.shard_map(
        local,
        mesh=mesh,
        in_specs=(P("sp", "tp"), P()) + (col,) * 10 + (P("tp"), P(), P("tp", None), P("tp", None)),
        out_specs=P(("sp", "tp"), None),
        check_vma=False,
    )
```

time: 236 us -> 86.8 us (0.37)
  waiting for transfers between devices: 99 us -> 0 us
  Pallas kernels: 0 us -> 75.5 us
  matrix products: 54.4 us -> 0 us
  blocking collectives: 19.9 us -> 0 us
  between operations: 14.3 us -> 0.75 us
  local copies, waits for them, and re-layouts: 23.5 us -> 10.1 us
  starting transfers between devices: 13 us -> 0 us
  other arithmetic: 9.27 us -> 0 us
    all_gather x1 -> x0, waiting for transfers between devices: 90.6 us -> none  [in_one_piece(): filled, at, outs = (lax.all_gather(both, axis, axis=dim, tiled=True), 0, [])]
    pallas_call x0 -> x1, Pallas kernels: none -> 75.5 us  [local(): pl.pallas_call(kernel, out_shape=jax.ShapeDtypeStruct((ROWS, D), BF), in_...]
    dot_general x35 -> x0, matrix products: 54.4 us -> none  [the longest x16 25 us: absorb(): jnp.einsum('hqk,khe->hqe', weights.astype(jnp.bfloat16), values, preferre...]
    all_to_all x1 -> x0, blocking collectives: 19.9 us -> none  [sum_at_owner(): lax.all_to_all(in_blocks(array, dim, devices), axis, 0, 0, tiled=True)]
    all_to_all x1 -> x0, starting transfers between devices: 10.4 us -> none  [from_everyone(): lax.all_to_all(jnp.broadcast_to(array[None], (devices, *array.shape)), ax...]
    slice x4 -> x0, local copies, waits for them, and re-layouts: 9.42 us -> none  [the longest x2 9.31 us: in_one_piece(): outs.append(lax.slice_in_dim(filled, at, at + a.shape[along], axis=along))]
    reduce_sum x19 -> x0, other arithmetic: 7.82 us -> none  [the longest x16 5.76 us: absorb(): totals = totals * factor + jnp.sum(weights, axis=2, keepdims=True)]
    concatenate x1 -> x0, local copies, waits for them, and re-layouts: 6.58 us -> none  [local(): stacked = jnp.concatenate(matrices, axis=1)]
  transfers between devices with their start and end apart: 4 -> 0, of which waited for: 3 -> 0; matrix products, arithmetic and copies ran while one was open for 4% -> 0% of each run, Pallas kernels for 0% -> 0%
where the time goes in v1:
time: 86.8 us; the launch traced here: 86.3 us
  Pallas kernels  75.5 us (87%)
  local copies, waits for them, and re-layouts  10.1 us (12%)
    pallas_call x1, Pallas kernels, local(): pl.pallas_call(kernel, out_shape=jax.ShapeDtypeStruct((ROWS, D), BF), in_...  75.5 us
    unnamed x33, local copies, waits for them, and re-layouts  10.1 us

profile of v1, /device:TPU:1, one launch (start us, length us, event | category | flops | bytes accessed | tf_op | source)
XLA Modules:
  0.0 86.3 jit_solution(5309124452343327649)
XLA Ops:
  0.7 0.0 copy-start.11
  0.7 1.3 %copy.17.wq1_h = bf16[2048,64]{1,0:T(8,128)(2,1)S(1)} copy(bf16[2048,64]{0,1:T(8,128)(2,1)} %param.18) | data formatting | bytes 524288 | tf_op args[2]
  1.9 0.0 copy-done.11
  1.9 0.0 copy-start.12
  2.0 0.3 copy.18.wk1_h
  2.2 0.7 copy-done.12
  2.9 0.0 copy-start.13
  2.9 0.0 copy-start.1
  2.9 0.3 copy.19.wq2_h
  3.2 0.7 copy-done.13
  3.8 0.0 copy-start
  3.8 0.0 copy-start.7
  3.9 0.0 copy-start.8
  3.9 0.0 copy-start.9
  3.9 0.0 copy-start.10
  3.9 0.3 copy.20.wk2_h
  4.1 0.0 copy-done.1
  4.2 0.8 copy-done
  4.9 0.0 copy-done.7
  4.9 0.0 copy-done.8
  5.0 0.0 copy-done.9
  5.0 0.0 copy-done.10
  5.0 0.0 copy-start.2
  5.0 1.0 %copy-done.2 = bf16[2048,128]{1,0:T(8,128)(2,1)S(1)} copy-done((bf16[2048,128]{1,0:T(8,128)(2,1)S(1)}, bf16[2048,128]{1,0:T(8,128)(2,1)}, u32[]{:S(2)}) %copy-start.2) | copy-done | bytes 524312
  6.0 0.0 copy-start.3
  6.0 1.0 %copy-done.3 = bf16[2048,128]{1,0:T(8,128)(2,1)S(1)} copy-done((bf16[2048,128]{1,0:T(8,128)(2,1)S(1)}, bf16[2048,128]{1,0:T(8,128)(2,1)}, u32[]{:S(2)}) %copy-start.3) | copy-done | bytes 524312
  7.0 0.0 copy-start.4
  7.0 1.0 %copy-done.4 = bf16[2048,128]{1,0:T(8,128)(2,1)S(1)} copy-done((bf16[2048,128]{1,0:T(8,128)(2,1)S(1)}, bf16[2048,128]{1,0:T(8,128)(2,1)}, u32[]{:S(2)}) %copy-start.4) | copy-done | bytes 524312
  8.1 0.0 copy-start.5
  8.1 1.0 %copy-done.5 = bf16[128,2048]{1,0:T(8,128)(2,1)S(1)} copy-done((bf16[128,2048]{1,0:T(8,128)(2,1)S(1)}, bf16[128,2048]{1,0:T(8,128)(2,1)}, u32[]{:S(2)}) %copy-start.5) | copy-done | bytes 524312
  9.1 0.0 copy-start.6
  9.1 1.0 %copy-done.6 = bf16[128,2048]{1,0:T(8,128)(2,1)S(1)} copy-done((bf16[128,2048]{1,0:T(8,128)(2,1)S(1)}, bf16[128,2048]{1,0:T(8,128)(2,1)}, u32[]{:S(2)}) %copy-start.6) | copy-done | bytes 524312
  10.2 75.5 %layer.1 = bf16[32,2048]{1,0:T(8,128)(2,1)S(1)} custom-call(bf16[256,256]{1,0:T(8,128)(2,1)S(1)} %copy-done.7, f32[1,2048]{1,0:T(1,128)S(1)} %bitcast.2, bf16[2048,64]{1,0:T(8,128)(2,1)S(1)} %copy.17.wq1_h, bf16[2048,64]{1,0:T(8,128)(2,1)S(1)} %copy.18.wk1_h, bf16[2048,64]{1,0:T(8,128)(2,1)S(1)} %copy.19.wq2_h, bf16[2048,64]{1,0:T(8,128)(2,1)S(1)} %copy.20.wk2_h, ...), custom_call_target="tpu_custom_call" | custom-call | tf_op jit(solution)/shard_map/layer/pallas_call | solution.py:357
  85.7 0.7 copy.23
Async XLA Ops:
  0.7 1.3 %copy-start.11 = (bf16[2048,64]{0,1:T(8,128)(2,1)S(1)}, bf16[2048,64]{0,1:T(8,128)(2,1)}, u32[]{:S(2)}) copy-start(bf16[2048,64]{0,1:T(8,128)(2,1)} %param.19) | copy-start | bytes 786436
  1.9 1.0 %copy-start.12 = (bf16[2048,64]{0,1:T(8,128)(2,1)S(1)}, bf16[2048,64]{0,1:T(8,128)(2,1)}, u32[]{:S(2)}) copy-start(bf16[2048,64]{0,1:T(8,128)(2,1)} %param.20) | copy-start | bytes 786436
  2.9 0.9 %copy-start.13 = (bf16[2048,64]{0,1:T(8,128)(2,1)S(1)}, bf16[2048,64]{0,1:T(8,128)(2,1)}, u32[]{:S(2)}) copy-start(bf16[2048,64]{0,1:T(8,128)(2,1)} %param.21) | copy-start | bytes 786436
  2.9 1.3 %copy-start.1 = (bf16[2048,128]{1,0:T(8,128)(2,1)S(1)}, bf16[2048,128]{1,0:T(8,128)(2,1)}, u32[]{:S(2)}) copy-start(bf16[2048,128]{1,0:T(8,128)(2,1)} %wg_h.1) | copy-start | bytes 1572868
  3.8 1.1 %copy-start = (bf16[2048,128]{1,0:T(8,128)(2,1)S(1)}, bf16[2048,128]{1,0:T(8,128)(2,1)}, u32[]{:S(2)}) copy-start(bf16[2048,128]{1,0:T(8,128)(2,1)} %wv_h.1) | copy-start | bytes 1572868
  3.8 1.1 %copy-start.7 = (bf16[256,256]{1,0:T(8,128)(2,1)S(1)}, bf16[256,256]{1,0:T(8,128)(2,1)}, u32[]{:S(2)}) copy-start(bf16[256,256]{1,0:T(8,128)(2,1)} %tok_h.1) | copy-start | bytes 393220
  3.9 1.1 %copy-start.8 = (f32[2048]{0:T(1024)S(1)}, f32[2048]{0:T(1024)}, u32[]{:S(2)}) copy-start(f32[2048]{0:T(1024)} %param.17) | copy-start | bytes 24580
  3.9 1.1 %copy-start.9 = (bf16[3,128]{1,0:T(4,128)(2,1)S(1)}, bf16[3,128]{1,0:T(4,128)(2,1)}, u32[]{:S(2)}) copy-start(bf16[3,128]{1,0:T(4,128)(2,1)} %taps.1) | copy-start | bytes 2308
  3.9 1.1 %copy-start.10 = (f32[128]{0:T(128)S(1)}, f32[128]{0:T(128)}, u32[]{:S(2)}) copy-start(f32[128]{0:T(128)} %param.29) | copy-start | bytes 1540
  5.0 1.0 %copy-start.2 = (bf16[2048,128]{1,0:T(8,128)(2,1)S(1)}, bf16[2048,128]{1,0:T(8,128)(2,1)}, u32[]{:S(2)}) copy-start(bf16[2048,128]{1,0:T(8,128)(2,1)} %wo_h.1) | copy-start | bytes 1572868
  6.0 1.0 %copy-start.3 = (bf16[2048,128]{1,0:T(8,128)(2,1)S(1)}, bf16[2048,128]{1,0:T(8,128)(2,1)}, u32[]{:S(2)}) copy-start(bf16[2048,128]{1,0:T(8,128)(2,1)} %wi_h.1) | copy-start | bytes 1572868
  7.0 1.0 %copy-start.4 = (bf16[2048,128]{1,0:T(8,128)(2,1)S(1)}, bf16[2048,128]{1,0:T(8,128)(2,1)}, u32[]{:S(2)}) copy-start(bf16[2048,128]{1,0:T(8,128)(2,1)} %wx_h.1) | copy-start | bytes 1572868
  8.1 1.0 %copy-start.5 = (bf16[128,2048]{1,0:T(8,128)(2,1)S(1)}, bf16[128,2048]{1,0:T(8,128)(2,1)}, u32[]{:S(2)}) copy-start(bf16[128,2048]{1,0:T(8,128)(2,1)} %aw_h.1) | copy-start | bytes 1572868
  9.1 1.0 %copy-start.6 = (bf16[128,2048]{1,0:T(8,128)(2,1)S(1)}, bf16[128,2048]{1,0:T(8,128)(2,1)}, u32[]{:S(2)}) copy-start(bf16[128,2048]{1,0:T(8,128)(2,1)} %cw_h.1) | copy-start | bytes 1572868

commit v2 on v1

--- a/solution.py
+++ b/solution.py
@@ -60,9 +60,9 @@
     cp_tok.start()
     loads = []
     for i, w in enumerate((wq1_h, wq2_h, wk1_h, wk2_h)):
-        loads.append(pltpu.make_async_copy(w, wn.at[i], lsem.at[1 + i]))
+        loads.append(pltpu.make_async_copy(w, wn.at[pl.ds(KD * i, KD), :], lsem.at[1 + i]))
     for i, w in enumerate((wv_h, wg_h, wo_h, wi_h, wx_h)):
-        loads.append(pltpu.make_async_copy(w, wall.at[:, pl.ds(256 + 128 * i, 128)], lsem.at[5 + i]))
+        loads.append(pltpu.make_async_copy(w, wall.at[:, pl.ds(128 * i, 128)], lsem.at[5 + i]))
     my_half = pl.ds(pl.multiple_of(c * HALF, HALF), HALF)
     other_half = pl.ds(pl.multiple_of((1 - c) * HALF, HALF), HALF)
     loads.append(pltpu.make_async_copy(aw_h.at[:, my_half], wout.at[c, pl.ds(0, VD), :], lsem.at[10]))
@@ -75,98 +75,150 @@
     def greet(dev):
         pl.semaphore_signal(barrier, inc=1, device_id=dev, device_id_type=MESH)
 
-    for d in range(1, 8):
-        greet((sp, (tp + d) % 8))
-        greet(kdev((kpos + d) % 8))
-        greet(qdev((qpos + d) % 8))
-    greet((prev_sp, tp))
-    greet((next_sp, tp))
-    pl.semaphore_wait(barrier, 23)
+    right_chip = (sp, ((x + 1) % 4) * 2 + c)
+    left_chip = (sp, ((x + 3) % 4) * 2 + c)
+    partner = (sp, other)
+    k_right, k_left = kdev((kpos + 1) % 8), kdev((kpos + 7) % 8)
+    q_right, q_left = qdev((qpos + 1) % 8), qdev((qpos + 7) % 8)
+    greeted = (right_chip, left_chip, partner, k_right, k_left, q_right, q_left, (prev_sp, tp), (next_sp, tp))
+    for dev in greeted:
+        greet(dev)
+    pl.semaphore_wait(barrier, len(greeted))
+
+    pending = []
+
+    def send(src, dst, ssem, rsem, dev):
+        cp = remote(src, dst, ssem, rsem, dev)
+        cp.start()
+        pending.append(cp)
+
+    def arrived(ref, rsem):
+        remote(ref, ref, rsem, rsem, partner).wait_recv()
+
+    top, bottom = pl.ds(0, T // 2), pl.ds(T // 2, T // 2)
+    halves = (top, bottom)
+
+    def tok_send(t, half, slot, dev):
+        ref = tok.at[t, halves[half], :]
+        send(ref, ref, tok_s.at[slot], tok_r.at[t, half], dev)
+
+    def tok_wait(t, half):
+        arrived(tok.at[t, halves[half], :], tok_r.at[t, half])
 
     cp_tok.wait()
-
-    def tok_to(j):
-        return remote(tok.at[tp], tok.at[tp], tok_s.at[j], tok_r.at[tp], (sp, ((x + j) % 4) * 2 + c))
-
-    def tok_fwd(t, slot):
-        return remote(tok.at[t], tok.at[t], tok_s.at[slot], tok_r.at[t], (sp, other))
-
-    tok_to(2).start()
-    tok_to(1).start()
-    tok_to(3).start()
-    tok_fwd(tp, 0).start()
-
-    wcopies = [
-        remote(aw_h.at[:, other_half], wout.at[c, pl.ds(0, VD), :], w_s.at[0], w_r.at[0], (sp, other)),
-        remote(cw_h.at[:, other_half], wout.at[c, pl.ds(VD, VD), :], w_s.at[1], w_r.at[1], (sp, other)),
-    ]
-    for cp in wcopies:
-        cp.start()
-
-    for cp in loads[:4]:
+    tok_send(tp, 0, 0, right_chip)
+    tok_send(tp, 1, 1, left_chip)
+    tok_send(tp, 1, 2, right_chip)
+    tok_send(tp, 0, 3, left_chip)
+    tok_send(tp, 0, 4, partner)
+    tok_send(tp, 1, 5, partner)
+
+    for cp in loads[:9]:
         cp.wait()
 
-    def join(i, carry):
-        rows = pl.ds(pl.multiple_of(i * 256, 256), 256)
-        wall[rows, pl.ds(0, 128)] = jnp.concatenate([wn[0, rows, :], wn[1, rows, :]], axis=1)
-        wall[rows, pl.ds(128, 128)] = jnp.concatenate([wn[2, rows, :], wn[3, rows, :]], axis=1)
-        return carry
-
-    lax.fori_loop(0, 8, join, 0)
-    for cp in loads[4:9]:
-        cp.wait()
-
-    acc[...] = jnp.zeros_like(acc)
-    ss[...] = jnp.zeros_like(ss)
-
-    def project(step, carry):
-        j = step // 2
-        odd = step % 2
-        dx = jnp.where(j == 0, 0, jnp.where(j == 1, 3, jnp.where(j == 2, 1, 2)))
-        chip = (x + dx) % 4
-        cc = (1 - odd) * c + odd * (1 - c)
-        t = chip * 2 + cc
-
-        @pl.when(step > 0)
-        def _():
-            remote(tok.at[t], tok.at[t], tok_s.at[0], tok_r.at[t], (sp, other)).wait_recv()
-
-        @pl.when((step > 1) & (odd == 0))
-        def _():
-            tok_fwd(t, 3 + j).start()
-
+    def project(t, first=False):
         block = tok[t].astype(F32)
         sq = block * block
-        ss[...] += sq[:, :128] + sq[:, 128:]
-        g = gain[:, pl.ds(pl.multiple_of(t * FB, FB), FB)]
-        scaled = (block * g).astype(BF)
-        acc[...] += dot(scaled, wall[pl.ds(pl.multiple_of(t * FB, FB), FB), :])
-        return carry
-
-    lax.fori_loop(0, 8, project, 0)
+        sq = sq[:, :128] + sq[:, 128:]
+        at = pl.ds(pl.multiple_of(t * FB, FB), FB)
+        scaled = (block * gain[:, at]).astype(BF)
+        narrow = lax.dot_general(scaled, wn[:, at], (((1,), (1,)), ((), ())), preferred_element_type=F32)
+        wide = dot(scaled, wall[at, :])
+        if first:
+            ss[...] = sq
+            acc[:, pl.ds(0, 256)] = narrow
+            acc[:, pl.ds(256, 640)] = wide
+        else:
+            ss[...] += sq
+            acc[:, pl.ds(0, 256)] += narrow
+            acc[:, pl.ds(256, 640)] += wide
+
+    xl, xr, xo = (x + 3) % 4, (x + 1) % 4, (x + 2) % 4
+    d = 1 - c
+    project(tp, True)
+    tok_wait(other, 0)
+    tok_wait(other, 1)
+    project(other)
+    tok_wait(xl * 2 + c, 0)
+    tok_send(xl * 2 + c, 0, 6, right_chip)
+    tok_send(xl * 2 + c, 0, 7, partner)
+    tok_wait(xr * 2 + c, 1)
+    tok_send(xr * 2 + c, 1, 8, left_chip)
+    tok_send(xr * 2 + c, 1, 9, partner)
+    tok_wait(xl * 2 + c, 1)
+    tok_send(xl * 2 + c, 1, 10, partner)
+    tok_wait(xr * 2 + c, 0)
+    tok_send(xr * 2 + c, 0, 11, partner)
+    project(xl * 2 + c)
+    project(xr * 2 + c)
+    tok_wait(xl * 2 + d, 0)
+    tok_wait(xl * 2 + d, 1)
+    project(xl * 2 + d)
+    tok_wait(xr * 2 + d, 0)
+    tok_wait(xr * 2 + d, 1)
+    project(xr * 2 + d)
+    tok_wait(xo * 2 + c, 0)
+    tok_send(xo * 2 + c, 0, 12, partner)
+    tok_wait(xo * 2 + c, 1)
+    tok_send(xo * 2 + c, 1, 13, partner)
+    project(xo * 2 + c)
+    tok_wait(xo * 2 + d, 0)
+    tok_wait(xo * 2 + d, 1)
+    project(xo * 2 + d)
 
     inv = lax.rsqrt(jnp.sum(ss[...], axis=1, keepdims=True) / D + EPS)
 
+    def k_send(pos, slot, dev):
+        send(kb.at[pos], kb.at[pos], k_s.at[slot], k_r.at[pos], dev)
+
+    def v_send(pos, slot, dev):
+        send(vb.at[pos], vb.at[pos], v_s.at[slot], v_r.at[pos], dev)
+
+    def q_send(pos, slot, dev):
+        send(qb.at[pos], qb.at[pos], q_s.at[slot], q_r.at[pos], dev)
+
+    def q_part(pos, part, slot, dev):
+        ref = qb.at[pos, pl.ds(KD * part, KD), :]
+        send(ref, ref, q_s.at[slot], q_r.at[pos if part == 0 else 8], dev)
+
     kb[kpos] = (acc[:, 128:256] * inv).astype(BF)
+    k_send(kpos, 0, k_right)
+    k_send(kpos, 1, k_left)
     vb[kpos] = (acc[:, 256:384] * inv).T.astype(BF)
+    v_send(kpos, 0, k_left)
+    v_send(kpos, 1, k_right)
     qb[qpos] = (acc[:, 0:128] * (inv * QSCALE)).T.astype(BF)
-
-    def k_to(d):
-        return remote(kb.at[kpos], kb.at[kpos], k_s.at[d], k_r.at[kpos], kdev((kpos + d) % 8))
-
-    def v_to(d):
-        return remote(vb.at[kpos], vb.at[kpos], v_s.at[d], v_r.at[kpos], kdev((kpos + d) % 8))
-
-    def q_to(d):
-        return remote(qb.at[qpos], qb.at[qpos], q_s.at[d], q_r.at[qpos], qdev((qpos + d) % 8))
-
-    order = (4, 3, 5, 2, 6, 1, 7)
-    for d in order:
-        k_to(d).start()
-    for d in order:
-        v_to(d).start()
-    for d in order:
-        q_to(d).start()
+    q_send(qpos, 0, q_right)
+    q_send(qpos, 1, q_left)
+
+    def ring_step(n):
+        kl, kr, ql, qr = (kpos + 8 - n) % 8, (kpos + n) % 8, (qpos + 8 - n) % 8, (qpos + n) % 8
+        arrived(kb.at[kl], k_r.at[kl])
+        if n < 4:
+            k_send(kl, 2 * n, k_right)
+            arrived(kb.at[kr], k_r.at[kr])
+            if n < 3:
+                k_send(kr, 2 * n + 1, k_left)
+        arrived(vb.at[kr], v_r.at[kr])
+        if n < 4:
+            v_send(kr, 2 * n, k_left)
+            arrived(vb.at[kl], v_r.at[kl])
+            if n < 3:
+                v_send(kl, 2 * n + 1, k_right)
+        if n < 4:
+            arrived(qb.at[ql], q_r.at[ql])
+            if n < 3:
+                q_send(ql, 2 * n, q_right)
+            else:
+                q_part(ql, 0, 6, q_right)
+            arrived(qb.at[qr], q_r.at[qr])
+            if n < 3:
+                q_send(qr, 2 * n + 1, q_left)
+            else:
+                q_part(qr, 1, 7, q_left)
+        else:
+            arrived(qb.at[ql, pl.ds(0, KD), :], q_r.at[ql])
+            arrived(qb.at[ql, pl.ds(KD, KD), :], q_r.at[8])
 
     gate[...] = (acc[:, 384:512] * inv).astype(BF)
     outer[...] = (acc[:, 512:640] * inv).astype(BF)
@@ -179,6 +231,7 @@
     to_next = remote(edge.at[1], halo.at[0], h_s.at[1], h_r.at[0], (next_sp, tp))
     to_prev.start()
     to_next.start()
+    ring_step(1)
     to_prev.wait_recv()
     to_next.wait_recv()
     before = jnp.where(sp == 0, 0.0, halo[0][7:8, :])
@@ -191,13 +244,11 @@
     conv = tp32[0:1] * up + tp32[1:2] * cur + tp32[2:3] * down
     mix[c, :, pl.ds(VD, VD)] = (outer[...].astype(F32) * conv).astype(BF)
 
-    def kv_wait(d, carry):
-        pos = (kpos + d) % 8
-        remote(kb.at[pos], kb.at[pos], k_s.at[0], k_r.at[pos], kdev(pos)).wait_recv()
-        remote(vb.at[pos], vb.at[pos], v_s.at[0], v_r.at[pos], kdev(pos)).wait_recv()
-        return carry
-
-    lax.fori_loop(1, 8, kv_wait, 0)
+    for n in (2, 3, 4):
+        ring_step(n)
+
+    send(aw_h.at[:, other_half], wout.at[c, pl.ds(0, VD), :], w_s.at[0], w_r.at[0], partner)
+    send(cw_h.at[:, other_half], wout.at[c, pl.ds(VD, VD), :], w_s.at[1], w_r.at[1], partner)
 
     zero = jnp.zeros((KD, T), BF)
 
@@ -218,10 +269,6 @@
         mag = 4 - (i + 1) // 2
         off = odd * mag + (1 - odd) * ((8 - mag) % 8)
         pos = (qpos + off) % 8
-
-        @pl.when(i < 7)
-        def _():
-            remote(qb.at[pos], qb.at[pos], q_s.at[0], q_r.at[pos], qdev(pos)).wait_recv()
 
         q = qb[pos]
         q1 = jnp.concatenate([q[:KD], zero], axis=0)
@@ -286,8 +333,8 @@
     share.start()
     for cp in loads[9:]:
         cp.wait()
-    for i in range(2):
-        wcopies[i].wait_recv()
+    arrived(wout.at[1 - c, pl.ds(0, VD), :], w_r.at[0])
+    arrived(wout.at[1 - c, pl.ds(VD, VD), :], w_r.at[1])
     share.wait_recv()
 
     def p_copy(chip, core):
@@ -328,14 +375,9 @@
             total += precv[2 * n + half].astype(F32)
         out[:, pl.ds(half * HALF, HALF)] = total.astype(BF)
 
-    tok_fwd(tp, 0).wait_send()
-    for j in (1, 2, 3):
-        tok_to(j).wait_send()
-        tok_fwd(tp, 3 + j).wait_send()
+    for cp in pending:
+        cp.wait_send()
     for d in range(1, 8):
-        k_to(d).wait_send()
-        v_to(d).wait_send()
-        q_to(d).wait_send()
         pos = (qpos + d) % 8
         remote(osend.at[pos], orecv.at[qpos], o_s.at[pos], o_r.at[qpos], qdev(pos)).wait_send()
         remote(tsend.at[pos], trecv.at[qpos], st_s.at[pos], st_r.at[qpos], qdev(pos)).wait_send()
@@ -344,12 +386,10 @@
     to_prev.wait_send()
     to_next.wait_send()
     share.wait_send()
-    for cp in wcopies:
-        cp.wait_send()
 
 
 def local(tokens, norm_gain, q1, k1, q2, k2, wv, wg, wo, wi, wx, taps, lam, hgain, aw, cw):
-    hbm = pl.BlockSpec(memory_space=pl.ANY)
+    hbm = pl.BlockSpec(memory_space=pltpu.HBM)
     vm = pl.BlockSpec(memory_space=pltpu.VMEM)
     sm = pl.BlockSpec(memory_space=pltpu.SMEM)
     dma = pltpu.SemaphoreType.DMA
@@ -360,21 +400,21 @@
         in_specs=[hbm, vm] + [hbm] * 9 + [vm, sm, vm, hbm, hbm],
         out_specs=vm,
         scratch_shapes=[
-            v((8, T, FB), BF), v((4, D, KD), BF), v((D, 896), BF), v((T, 896), F32), v((T, 128), F32),
+            v((8, T, FB), BF), v((4 * KD, D), BF), v((D, 640), BF), v((T, 896), F32), v((T, 128), F32),
             v((R, T, 128), BF), v((R, VD, T), BF), v((R, 128, T), BF),
             v((T, VD), BF), v((T, VD), BF), v((T, VD), F32), v((2, 8, VD), F32), v((2, 8, VD), F32),
             v((KEYS, T), F32), v((KEYS, T), F32),
             v((R, 2 * VD, T), BF), v((R, 2 * VD, T), BF), v((R, 8, T), F32), v((R, 8, T), F32),
             v((2, T, 2 * VD), BF), v((2, 2 * VD, HALF), BF), v((4, 2 * ROWS, HALF), BF), v((8, ROWS, HALF), BF),
-            dma((12,)), dma((8,)), dma((8,)), dma((8,)), dma((8,)), dma((8,)), dma((8,)), dma((8,)), dma((8,)),
+            dma((12,)), dma((14,)), dma((8, 2)), dma((8,)), dma((8,)), dma((8,)), dma((8,)), dma((8,)), dma((9,)),
             dma((8,)), dma((8,)), dma((8,)), dma((8,)), dma((2,)), dma((2,)), dma, dma, dma((2,)), dma((2,)),
             dma((8,)), dma((8,)),
         ],
         compiler_params=pltpu.CompilerParams(
-            collective_id=0, has_side_effects=True, vmem_limit_bytes=48 * 1024 * 1024
+            collective_id=0, has_side_effects=True, vmem_limit_bytes=67043328
         ),
         name="layer",
-    )(tokens, norm_gain.reshape(1, D), q1, k1, q2, k2, wv, wg, wo, wi, wx, taps, lam, hgain.reshape(1, VD), aw, cw)
+    )(tokens, norm_gain.reshape(1, D), q1.T, k1.T, q2.T, k2.T, wv, wg, wo, wi, wx, taps, lam, hgain.reshape(1, VD), aw, cw)
 
 
 def solution(mesh):

time: 86.8 us -> 71.6 us (0.82)
  local copies, waits for them, and re-layouts: 10.1 us -> 1.57 us
  Pallas kernels: 75.5 us -> 69.1 us
    unnamed x33 -> x1, local copies, waits for them, and re-layouts: 10.1 us -> 1.57 us
    pallas_call x1, Pallas kernels: 75.5 us -> 69.1 us  [local(): pl.pallas_call(kernel, out_shape=jax.ShapeDtypeStruct((ROWS, D), BF), in_...]
where the time goes in v2:
time: 71.6 us; the launch traced here: 71.4 us
  Pallas kernels  69.1 us (97%)
  local copies, waits for them, and re-layouts  1.57 us (2%)
    pallas_call x1, Pallas kernels, local(): pl.pallas_call(kernel, out_shape=jax.ShapeDtypeStruct((ROWS, D), BF), in_...  69.1 us
    unnamed x1, local copies, waits for them, and re-layouts  1.57 us

profile of v2, /device:TPU:1, one launch (start us, length us, event | category | flops | bytes accessed | tf_op | source)
XLA Modules:
  0.0 71.4 jit_solution(14383388013117348258)
XLA Ops:
  0.7 69.1 %layer.1 = bf16[32,2048]{1,0:T(8,128)(2,1)} custom-call(bf16[256,256]{1,0:T(8,128)(2,1)} %tok_h.1, f32[1,2048]{1,0:T(1,128)} %bitcast.10, bf16[64,2048]{1,0:T(8,128)(2,1)} %bitcast.6, bf16[64,2048]{1,0:T(8,128)(2,1)} %bitcast.7, bf16[64,2048]{1,0:T(8,128)(2,1)} %bitcast.8, bf16[64,2048]{1,0:T(8,128)(2,1)} %bitcast.9, bf16[2048,128]{1,0:T(8,128)(2,1)} %wv_h.1, ...), custom_call_target="tpu_custom_call" | custom-call | tf_op jit(solution)/shard_map/layer/pallas_call | solution.py:397
  69.8 1.6 %copy.19 = bf16[32,2048]{1,0:T(8,128)(2,1)} copy(bf16[32,2048]{1,0:T(8,128)(2,1)} %layer.1) | data formatting | bytes 262144

commit v3 on v2

--- a/solution.py
+++ b/solution.py
@@ -27,8 +27,8 @@
     tok_h, gain, wq1_h, wk1_h, wq2_h, wk2_h, wv_h, wg_h, wo_h, wi_h, wx_h, taps, lam, hgain, aw_h, cw_h,
     out,
     tok, wn, wall, acc, ss, kb, vb, qb, gate, outer, prod, edge, halo, s1, s2, osend, orecv, tsend, trecv,
-    mix, wout, psend, precv,
-    lsem, tok_s, tok_r, k_s, k_r, v_s, v_r, q_s, q_r, o_s, o_r, st_s, st_r, h_s, h_r, m_s, m_r, w_s, w_r, p_s, p_r,
+    mix, wout, psend, precv, wa, csum, amix, arecv,
+    lsem, tok_s, tok_r, k_s, k_r, v_s, v_r, q_s, q_r, o_s, o_r, st_s, st_r, h_s, h_r, m_s, m_r, w_s, w_r, p_s, p_r, wa_s, wa_r, a_s, a_r,
 ):
     sp = lax.axis_index("sp")
     tp = lax.axis_index("tp")
@@ -65,8 +65,8 @@
         loads.append(pltpu.make_async_copy(w, wall.at[:, pl.ds(128 * i, 128)], lsem.at[5 + i]))
     my_half = pl.ds(pl.multiple_of(c * HALF, HALF), HALF)
     other_half = pl.ds(pl.multiple_of((1 - c) * HALF, HALF), HALF)
-    loads.append(pltpu.make_async_copy(aw_h.at[:, my_half], wout.at[c, pl.ds(0, VD), :], lsem.at[10]))
-    loads.append(pltpu.make_async_copy(cw_h.at[:, my_half], wout.at[c, pl.ds(VD, VD), :], lsem.at[11]))
+    loads.append(pltpu.make_async_copy(aw_h, wa.at[pl.ds(pl.multiple_of(tp * VD, VD), VD), :], lsem.at[10]))
+    loads.append(pltpu.make_async_copy(cw_h.at[:, my_half], wout.at[c], lsem.at[11]))
     for cp in loads:
         cp.start()
 
@@ -80,7 +80,12 @@
     partner = (sp, other)
     k_right, k_left = kdev((kpos + 1) % 8), kdev((kpos + 7) % 8)
     q_right, q_left = qdev((qpos + 1) % 8), qdev((qpos + 7) % 8)
-    greeted = (right_chip, left_chip, partner, k_right, k_left, q_right, q_left, (prev_sp, tp), (next_sp, tp))
+    k_right2, k_left2 = kdev((kpos + 2) % 8), kdev((kpos + 6) % 8)
+    q_right2, q_left2 = qdev((qpos + 2) % 8), qdev((qpos + 6) % 8)
+    greeted = (
+        right_chip, left_chip, partner, (prev_sp, tp), (next_sp, tp),
+        k_right, k_left, q_right, q_left, k_right2, k_left2, q_right2, q_left2,
+    )
     for dev in greeted:
         greet(dev)
     pl.semaphore_wait(barrier, len(greeted))
@@ -134,7 +139,7 @@
             acc[:, pl.ds(256, 640)] += wide
 
     xl, xr, xo = (x + 3) % 4, (x + 1) % 4, (x + 2) % 4
-    d = 1 - c
+    oc = 1 - c
     project(tp, True)
     tok_wait(other, 0)
     tok_wait(other, 1)
@@ -151,20 +156,43 @@
     tok_send(xr * 2 + c, 0, 11, partner)
     project(xl * 2 + c)
     project(xr * 2 + c)
-    tok_wait(xl * 2 + d, 0)
-    tok_wait(xl * 2 + d, 1)
-    project(xl * 2 + d)
-    tok_wait(xr * 2 + d, 0)
-    tok_wait(xr * 2 + d, 1)
-    project(xr * 2 + d)
+    tok_wait(xl * 2 + oc, 0)
+    tok_wait(xl * 2 + oc, 1)
+    project(xl * 2 + oc)
+    tok_wait(xr * 2 + oc, 0)
+    tok_wait(xr * 2 + oc, 1)
+    project(xr * 2 + oc)
     tok_wait(xo * 2 + c, 0)
     tok_send(xo * 2 + c, 0, 12, partner)
     tok_wait(xo * 2 + c, 1)
     tok_send(xo * 2 + c, 1, 13, partner)
     project(xo * 2 + c)
-    tok_wait(xo * 2 + d, 0)
-    tok_wait(xo * 2 + d, 1)
-    project(xo * 2 + d)
+    tok_wait(xo * 2 + oc, 0)
+    tok_wait(xo * 2 + oc, 1)
+    project(xo * 2 + oc)
+
+    quarter = VD // 2
+
+    def wa_part(t, half):
+        return wa.at[pl.ds(pl.multiple_of(t * VD + half * quarter, quarter), quarter), :]
+
+    def wa_copy(t, half, slot, dev):
+        return remote(wa_part(t, half), wa_part(t, half), wa_s.at[slot], wa_r.at[t, half], dev)
+
+    def wa_send(t, half, slot, dev):
+        send(wa_part(t, half), wa_part(t, half), wa_s.at[slot], wa_r.at[t, half], dev)
+
+    def wa_wait(t, half):
+        arrived(wa_part(t, half), wa_r.at[t, half])
+
+    for cp in loads[9:]:
+        cp.wait()
+    wa_send(tp, 0, 0, right_chip)
+    wa_send(tp, 1, 1, left_chip)
+    wa_send(tp, 1, 2, right_chip)
+    wa_send(tp, 0, 3, left_chip)
+    wa_send(tp, 0, 4, partner)
+    wa_send(tp, 1, 5, partner)
 
     inv = lax.rsqrt(jnp.sum(ss[...], axis=1, keepdims=True) / D + EPS)
 
@@ -182,43 +210,14 @@
         send(ref, ref, q_s.at[slot], q_r.at[pos if part == 0 else 8], dev)
 
     kb[kpos] = (acc[:, 128:256] * inv).astype(BF)
-    k_send(kpos, 0, k_right)
-    k_send(kpos, 1, k_left)
+    for slot, dev in enumerate((k_right2, k_left2, k_right, k_left)):
+        k_send(kpos, slot, dev)
     vb[kpos] = (acc[:, 256:384] * inv).T.astype(BF)
-    v_send(kpos, 0, k_left)
-    v_send(kpos, 1, k_right)
+    for slot, dev in enumerate((k_left2, k_right2, k_left, k_right)):
+        v_send(kpos, slot, dev)
     qb[qpos] = (acc[:, 0:128] * (inv * QSCALE)).T.astype(BF)
-    q_send(qpos, 0, q_right)
-    q_send(qpos, 1, q_left)
-
-    def ring_step(n):
-        kl, kr, ql, qr = (kpos + 8 - n) % 8, (kpos + n) % 8, (qpos + 8 - n) % 8, (qpos + n) % 8
-        arrived(kb.at[kl], k_r.at[kl])
-        if n < 4:
-            k_send(kl, 2 * n, k_right)
-            arrived(kb.at[kr], k_r.at[kr])
-            if n < 3:
-                k_send(kr, 2 * n + 1, k_left)
-        arrived(vb.at[kr], v_r.at[kr])
-        if n < 4:
-            v_send(kr, 2 * n, k_left)
-            arrived(vb.at[kl], v_r.at[kl])
-            if n < 3:
-                v_send(kl, 2 * n + 1, k_right)
-        if n < 4:
-            arrived(qb.at[ql], q_r.at[ql])
-            if n < 3:
-                q_send(ql, 2 * n, q_right)
-            else:
-                q_part(ql, 0, 6, q_right)
-            arrived(qb.at[qr], q_r.at[qr])
-            if n < 3:
-                q_send(qr, 2 * n + 1, q_left)
-            else:
-                q_part(qr, 1, 7, q_left)
-        else:
-            arrived(qb.at[ql, pl.ds(0, KD), :], q_r.at[ql])
-            arrived(qb.at[ql, pl.ds(KD, KD), :], q_r.at[8])
+    for slot, dev in enumerate((q_right2, q_left2, q_right, q_left)):
+        q_send(qpos, slot, dev)
 
     gate[...] = (acc[:, 384:512] * inv).astype(BF)
     outer[...] = (acc[:, 512:640] * inv).astype(BF)
@@ -231,7 +230,26 @@
     to_next = remote(edge.at[1], halo.at[0], h_s.at[1], h_r.at[0], (next_sp, tp))
     to_prev.start()
     to_next.start()
-    ring_step(1)
+
+    def at(pos, d):
+        return (pos + d) % 8
+
+    arrived(kb.at[at(kpos, 6)], k_r.at[at(kpos, 6)])
+    k_send(at(kpos, 6), 4, k_right2)
+    k_send(at(kpos, 6), 5, k_right)
+    arrived(kb.at[at(kpos, 2)], k_r.at[at(kpos, 2)])
+    k_send(at(kpos, 2), 6, k_left)
+    arrived(vb.at[at(kpos, 2)], v_r.at[at(kpos, 2)])
+    v_send(at(kpos, 2), 4, k_left2)
+    v_send(at(kpos, 2), 5, k_left)
+    arrived(vb.at[at(kpos, 6)], v_r.at[at(kpos, 6)])
+    v_send(at(kpos, 6), 6, k_right)
+    arrived(qb.at[at(qpos, 6)], q_r.at[at(qpos, 6)])
+    q_part(at(qpos, 6), 0, 4, q_right2)
+    q_send(at(qpos, 6), 5, q_right)
+    arrived(qb.at[at(qpos, 2)], q_r.at[at(qpos, 2)])
+    q_part(at(qpos, 2), 1, 6, q_left2)
+    q_send(at(qpos, 2), 7, q_left)
     to_prev.wait_recv()
     to_next.wait_recv()
     before = jnp.where(sp == 0, 0.0, halo[0][7:8, :])
@@ -242,13 +260,53 @@
     down = jnp.where(rows == T - 1, after, pltpu.roll(cur, T - 1, 0))
     tp32 = taps[...].astype(F32)
     conv = tp32[0:1] * up + tp32[1:2] * cur + tp32[2:3] * down
-    mix[c, :, pl.ds(VD, VD)] = (outer[...].astype(F32) * conv).astype(BF)
-
-    for n in (2, 3, 4):
-        ring_step(n)
-
-    send(aw_h.at[:, other_half], wout.at[c, pl.ds(0, VD), :], w_s.at[0], w_r.at[0], partner)
-    send(cw_h.at[:, other_half], wout.at[c, pl.ds(VD, VD), :], w_s.at[1], w_r.at[1], partner)
+    mix[c] = (outer[...].astype(F32) * conv).astype(BF)
+
+    send(mix.at[c], mix.at[c], m_s, m_r, partner)
+    send(cw_h.at[:, other_half], wout.at[c], w_s, w_r, partner)
+    arrived(mix.at[1 - c], m_r)
+    arrived(wout.at[1 - c], w_r)
+
+    def p_copy(chip, core):
+        return remote(
+            psend.at[chip, pl.ds(pl.multiple_of(core * ROWS, ROWS), ROWS), :],
+            precv.at[tp],
+            p_s.at[chip * 2 + core],
+            p_r.at[tp],
+            (sp, chip * 2 + core),
+        )
+
+    def to_chip(i, carry):
+        chip = (x + jnp.where(i == 0, 2, jnp.where(i == 1, 1, jnp.where(i == 2, 3, 0)))) % 4
+        rows = pl.ds(pl.multiple_of(chip * 2 * ROWS, 2 * ROWS), 2 * ROWS)
+        psend[chip] = (dot(mix[0, rows, :], wout[0]) + dot(mix[1, rows, :], wout[1])).astype(BF)
+
+        @pl.when(i < 3)
+        def _():
+            p_copy(chip, c).start()
+
+        p_copy(chip, 1 - c).start()
+        return carry
+
+    lax.fori_loop(0, 4, to_chip, 0)
+    precv[tp] = psend[x, pl.ds(pl.multiple_of(c * ROWS, ROWS), ROWS), :]
+
+    for d in (1, 7, 3, 5, 4):
+        arrived(kb.at[at(kpos, d)], k_r.at[at(kpos, d)])
+        arrived(vb.at[at(kpos, d)], v_r.at[at(kpos, d)])
+    for d in (1, 7, 3, 5):
+        arrived(qb.at[at(qpos, d)], q_r.at[at(qpos, d)])
+    arrived(qb.at[at(qpos, 4), pl.ds(0, KD), :], q_r.at[at(qpos, 4)])
+    arrived(qb.at[at(qpos, 4), pl.ds(KD, KD), :], q_r.at[8])
+
+    def wa_forward():
+        for slot, (t, half, dev) in enumerate((
+            (xl * 2 + c, 0, right_chip), (xr * 2 + c, 1, left_chip), (xl * 2 + c, 1, None), (xr * 2 + c, 0, None)
+        )):
+            wa_wait(t, half)
+            if dev is not None:
+                wa_copy(t, half, 6 + slot, dev).start()
+            wa_copy(t, half, 8 + slot, partner).start()
 
     zero = jnp.zeros((KD, T), BF)
 
@@ -269,6 +327,8 @@
         mag = 4 - (i + 1) // 2
         off = odd * mag + (1 - odd) * ((8 - mag) % 8)
         pos = (qpos + off) % 8
+
+        pl.when(i == 2)(wa_forward)
 
         q = qb[pos]
         q1 = jnp.concatenate([q[:KD], zero], axis=0)
@@ -304,6 +364,26 @@
     orecv[qpos] = osend[qpos]
     trecv[qpos] = tsend[qpos]
 
+    wa_wait(xo * 2 + c, 0)
+    wa_send(xo * 2 + c, 0, 12, partner)
+    wa_wait(xo * 2 + c, 1)
+    wa_send(xo * 2 + c, 1, 13, partner)
+
+    def p_wait(d, carry):
+        src = (tp + d) % 8
+        arrived(precv.at[src], p_r.at[src])
+        return carry
+
+    lax.fori_loop(1, 8, p_wait, 0)
+    for half in range(2):
+        total = precv[half].astype(F32)
+        for n in range(1, 4):
+            total += precv[2 * n + half].astype(F32)
+        csum[:, pl.ds(half * HALF, HALF)] = total
+    for t in (other, xl * 2 + oc, xr * 2 + oc, xo * 2 + oc):
+        wa_wait(t, 0)
+        wa_wait(t, 1)
+
     def o_wait(d, carry):
         pos = (qpos + d) % 8
         remote(osend.at[pos], orecv.at[pos], o_s.at[pos], o_r.at[pos], qdev(pos)).wait_recv()
@@ -327,65 +407,37 @@
     diff = merged(0, 0) - lam[0] * merged(2, VD)
     diff = (diff * lax.rsqrt(jnp.mean(diff * diff, axis=0, keepdims=True) + EPS)).T
     g32 = gate[...].astype(F32)
-    mix[c, :, pl.ds(0, VD)] = (diff * hgain[...] * (g32 / (1.0 + jnp.exp(-g32)))).astype(BF)
-
-    share = remote(mix.at[c], mix.at[c], m_s, m_r, (sp, other))
-    share.start()
-    for cp in loads[9:]:
-        cp.wait()
-    arrived(wout.at[1 - c, pl.ds(0, VD), :], w_r.at[0])
-    arrived(wout.at[1 - c, pl.ds(VD, VD), :], w_r.at[1])
-    share.wait_recv()
-
-    def p_copy(chip, core):
-        return remote(
-            psend.at[chip, pl.ds(pl.multiple_of(core * ROWS, ROWS), ROWS), :],
-            precv.at[tp],
-            p_s.at[chip * 2 + core],
-            p_r.at[tp],
-            (sp, chip * 2 + core),
-        )
-
-    def to_chip(i, carry):
-        chip = (x + jnp.where(i == 0, 2, jnp.where(i == 1, 1, jnp.where(i == 2, 3, 0)))) % 4
-        rows = pl.ds(pl.multiple_of(chip * 2 * ROWS, 2 * ROWS), 2 * ROWS)
-        psend[chip] = (dot(mix[0, rows, :], wout[0]) + dot(mix[1, rows, :], wout[1])).astype(BF)
-
-        @pl.when(i < 3)
-        def _():
-            p_copy(chip, c).start()
-
-        p_copy(chip, 1 - c).start()
-        return carry
-
-    lax.fori_loop(0, 4, to_chip, 0)
-    precv[tp] = psend[x, pl.ds(pl.multiple_of(c * ROWS, ROWS), ROWS), :]
-
-    def p_wait(d, carry):
-        src = (tp + d) % 8
-        remote(
-            psend.at[0, pl.ds(0, ROWS), :], precv.at[src], p_s.at[0], p_r.at[src], (sp, src)
-        ).wait_recv()
-        return carry
-
-    lax.fori_loop(1, 8, p_wait, 0)
-    for half in range(2):
-        total = precv[half].astype(F32)
-        for n in range(1, 4):
-            total += precv[2 * n + half].astype(F32)
-        out[:, pl.ds(half * HALF, HALF)] = total.astype(BF)
+    amix[...] = (diff * hgain[...] * (g32 / (1.0 + jnp.exp(-g32)))).astype(BF)
+
+    mine = pl.ds(pl.multiple_of(tp * VD, VD), VD)
+
+    def a_copy(t):
+        rows = pl.ds(pl.multiple_of(t * ROWS, ROWS), ROWS)
+        return remote(amix.at[rows, :], arecv.at[:, mine], a_s.at[t], a_r.at[tp], (sp, t))
+
+    for e in (4, 5, 3, 2, 6, 1, 7):
+        a_copy((tp + e) % 8).start()
+    arecv[:, mine] = amix[pl.ds(pl.multiple_of(tp * ROWS, ROWS), ROWS), :]
+    for e in (1, 7, 2, 6, 3, 5, 4):
+        src = (tp + e) % 8
+        arrived(arecv.at[:, pl.ds(pl.multiple_of(src * VD, VD), VD)], a_r.at[src])
+    for n in range(4):
+        cols = pl.ds(n * 512, 512)
+        out[:, cols] = (dot(arecv[...], wa[:, cols]) + csum[:, cols]).astype(BF)
 
     for cp in pending:
         cp.wait_send()
+    for slot in range(6, 12):
+        wa_copy(tp, 0, slot, partner).wait_send()
     for d in range(1, 8):
         pos = (qpos + d) % 8
         remote(osend.at[pos], orecv.at[qpos], o_s.at[pos], o_r.at[qpos], qdev(pos)).wait_send()
         remote(tsend.at[pos], trecv.at[qpos], st_s.at[pos], st_r.at[qpos], qdev(pos)).wait_send()
         dst = (tp + d) % 8
         p_copy(dst // 2, dst % 2).wait_send()
+        a_copy(dst).wait_send()
     to_prev.wait_send()
     to_next.wait_send()
-    share.wait_send()
 
 
 def local(tokens, norm_gain, q1, k1, q2, k2, wv, wg, wo, wi, wx, taps, lam, hgain, aw, cw):
@@ -405,10 +457,11 @@
             v((T, VD), BF), v((T, VD), BF), v((T, VD), F32), v((2, 8, VD), F32), v((2, 8, VD), F32),
             v((KEYS, T), F32), v((KEYS, T), F32),
             v((R, 2 * VD, T), BF), v((R, 2 * VD, T), BF), v((R, 8, T), F32), v((R, 8, T), F32),
-            v((2, T, 2 * VD), BF), v((2, 2 * VD, HALF), BF), v((4, 2 * ROWS, HALF), BF), v((8, ROWS, HALF), BF),
+            v((2, T, VD), BF), v((2, VD, HALF), BF), v((4, 2 * ROWS, HALF), BF), v((8, ROWS, HALF), BF),
+            v((8 * VD, D), BF), v((ROWS, D), F32), v((T, VD), BF), v((ROWS, 8 * VD), BF),
             dma((12,)), dma((14,)), dma((8, 2)), dma((8,)), dma((8,)), dma((8,)), dma((8,)), dma((8,)), dma((9,)),
-            dma((8,)), dma((8,)), dma((8,)), dma((8,)), dma((2,)), dma((2,)), dma, dma, dma((2,)), dma((2,)),
-            dma((8,)), dma((8,)),
+            dma((8,)), dma((8,)), dma((8,)), dma((8,)), dma((2,)), dma((2,)), dma, dma, dma, dma,
+            dma((8,)), dma((8,)), dma((14,)), dma((8, 2)), dma((8,)), dma((8,)),
         ],
         compiler_params=pltpu.CompilerParams(
             collective_id=0, has_side_effects=True, vmem_limit_bytes=67043328

time: 71.6 us -> 65 us (0.908)
  Pallas kernels: 69.1 us -> 62.6 us
    pallas_call x1, Pallas kernels: 69.1 us -> 62.6 us  [local(): pl.pallas_call(kernel, out_shape=jax.ShapeDtypeStruct((ROWS, D), BF), in_...]
where the time goes in v3:
time: 65 us; the launch traced here: 64.9 us
  Pallas kernels  62.6 us (96%)
  local copies, waits for them, and re-layouts  1.57 us (2%)
  between operations  0.66 us (1%)
    pallas_call x1, Pallas kernels, local(): pl.pallas_call(kernel, out_shape=jax.ShapeDtypeStruct((ROWS, D), BF), in_...  62.6 us
    unnamed x1, local copies, waits for them, and re-layouts  1.57 us

profile of v3, /device:TPU:1, one launch (start us, length us, event | category | flops | bytes accessed | tf_op | source)
XLA Modules:
  0.0 64.9 jit_solution(15634611340619589279)
XLA Ops:
  0.7 62.6 %layer.1 = bf16[32,2048]{1,0:T(8,128)(2,1)} custom-call(bf16[256,256]{1,0:T(8,128)(2,1)} %tok_h.1, f32[1,2048]{1,0:T(1,128)} %bitcast.10, bf16[64,2048]{1,0:T(8,128)(2,1)} %bitcast.6, bf16[64,2048]{1,0:T(8,128)(2,1)} %bitcast.7, bf16[64,2048]{1,0:T(8,128)(2,1)} %bitcast.8, bf16[64,2048]{1,0:T(8,128)(2,1)} %bitcast.9, bf16[2048,128]{1,0:T(8,128)(2,1)} %wv_h.1, ...), custom_call_target="tpu_custom_call" | custom-call | tf_op jit(solution)/shard_map/layer/pallas_call | solution.py:449
  63.3 1.6 %copy.19 = bf16[32,2048]{1,0:T(8,128)(2,1)} copy(bf16[32,2048]{1,0:T(8,128)(2,1)} %layer.1) | data formatting | bytes 262144

commit v4 on v3

--- a/solution.py
+++ b/solution.py
@@ -27,7 +27,7 @@
     tok_h, gain, wq1_h, wk1_h, wq2_h, wk2_h, wv_h, wg_h, wo_h, wi_h, wx_h, taps, lam, hgain, aw_h, cw_h,
     out,
     tok, wn, wall, acc, ss, kb, vb, qb, gate, outer, prod, edge, halo, s1, s2, osend, orecv, tsend, trecv,
-    mix, wout, psend, precv, wa, csum, amix, arecv,
+    mix, wout, psend, precv, wa, csum, amix, arecv, ms, mo,
     lsem, tok_s, tok_r, k_s, k_r, v_s, v_r, q_s, q_r, o_s, o_r, st_s, st_r, h_s, h_r, m_s, m_r, w_s, w_r, p_s, p_r, wa_s, wa_r, a_s, a_r,
 ):
     sp = lax.axis_index("sp")
@@ -291,6 +291,13 @@
     lax.fori_loop(0, 4, to_chip, 0)
     precv[tp] = psend[x, pl.ds(pl.multiple_of(c * ROWS, ROWS), ROWS), :]
 
+    wa_wait(xl * 2 + c, 0)
+    wa_send(xl * 2 + c, 0, 6, right_chip)
+    wa_send(xl * 2 + c, 0, 8, partner)
+    wa_wait(xr * 2 + c, 1)
+    wa_send(xr * 2 + c, 1, 7, left_chip)
+    wa_send(xr * 2 + c, 1, 9, partner)
+
     for d in (1, 7, 3, 5, 4):
         arrived(kb.at[at(kpos, d)], k_r.at[at(kpos, d)])
         arrived(vb.at[at(kpos, d)], v_r.at[at(kpos, d)])
@@ -300,13 +307,9 @@
     arrived(qb.at[at(qpos, 4), pl.ds(KD, KD), :], q_r.at[8])
 
     def wa_forward():
-        for slot, (t, half, dev) in enumerate((
-            (xl * 2 + c, 0, right_chip), (xr * 2 + c, 1, left_chip), (xl * 2 + c, 1, None), (xr * 2 + c, 0, None)
-        )):
+        for slot, (t, half) in enumerate(((xl * 2 + c, 1), (xr * 2 + c, 0))):
             wa_wait(t, half)
-            if dev is not None:
-                wa_copy(t, half, 6 + slot, dev).start()
-            wa_copy(t, half, 8 + slot, partner).start()
+            wa_copy(t, half, 10 + slot, partner).start()
 
     zero = jnp.zeros((KD, T), BF)
 
@@ -322,21 +325,21 @@
         o = dot(vb[n], p.astype(BF))
         return (part, o) if state is None else (state[0] + part, state[1] + o)
 
-    def one_block(i, carry):
+    def ring_place(i):
         odd = i % 2
         mag = 4 - (i + 1) // 2
-        off = odd * mag + (1 - odd) * ((8 - mag) % 8)
-        pos = (qpos + off) % 8
-
+        return (qpos + odd * mag + (1 - odd) * ((8 - mag) % 8)) % 8
+
+    def first_map(pos):
+        return jnp.concatenate([qb[pos, pl.ds(0, KD), :], zero], axis=0)
+
+    def second_map(pos):
+        return jnp.concatenate([zero, qb[pos, pl.ds(KD, KD), :]], axis=0)
+
+    def one_block(i, peak1):
+        pos = ring_place(i)
         pl.when(i == 2)(wa_forward)
-
-        q = qb[pos]
-        q1 = jnp.concatenate([q[:KD], zero], axis=0)
-        q2 = jnp.concatenate([zero, q[KD:]], axis=0)
-        peak = None
-        for n in range(R):
-            peak = scores(q1, n, s1, peak)
-        peak1 = jnp.max(peak, axis=0, keepdims=True)
+        q2 = second_map(pos)
         peak = None
         state = None
         for n in range(R):
@@ -345,9 +348,13 @@
         peak2 = jnp.max(peak, axis=0, keepdims=True)
         sum1 = jnp.sum(state[0], axis=0, keepdims=True)
         osend[pos, pl.ds(0, VD), :] = state[1].astype(BF)
+        q1 = first_map(ring_place((i + 1) % 8))
+        peak = None
         state = None
         for n in range(R):
+            peak = scores(q1, n, s1, peak)
             state = apply(n, s2, peak2, state)
+        next1 = jnp.max(peak, axis=0, keepdims=True)
         sum2 = jnp.sum(state[0], axis=0, keepdims=True)
         osend[pos, pl.ds(VD, VD), :] = state[1].astype(BF)
         tsend[pos] = jnp.concatenate([peak1, sum1, peak2, sum2, peak1, sum1, peak2, sum2], axis=0)
@@ -357,9 +364,13 @@
             remote(osend.at[pos], orecv.at[qpos], o_s.at[pos], o_r.at[qpos], qdev(pos)).start()
             remote(tsend.at[pos], trecv.at[qpos], st_s.at[pos], st_r.at[qpos], qdev(pos)).start()
 
-        return carry
-
-    lax.fori_loop(0, 8, one_block, 0)
+        return next1
+
+    q1 = first_map(ring_place(0))
+    peak = None
+    for n in range(R):
+        peak = scores(q1, n, s1, peak)
+    lax.fori_loop(0, 8, one_block, jnp.max(peak, axis=0, keepdims=True))
 
     orecv[qpos] = osend[qpos]
     trecv[qpos] = tsend[qpos]
@@ -384,27 +395,37 @@
         wa_wait(t, 0)
         wa_wait(t, 1)
 
-    def o_wait(d, carry):
+    def part(n):
+        t = trecv[n]
+        return [
+            (t[2 * m : 2 * m + 1], t[2 * m + 1 : 2 * m + 2], orecv[n, pl.ds(m * VD, VD), :].astype(F32))
+            for m in range(2)
+        ]
+
+    def merge(a, b):
+        peak = jnp.maximum(a[0], b[0])
+        wa_, wb_ = jnp.exp2(a[0] - peak), jnp.exp2(b[0] - peak)
+        return peak, wa_ * a[1] + wb_ * b[1], wa_ * a[2] + wb_ * b[2]
+
+    def take(d, state):
         pos = (qpos + d) % 8
-        remote(osend.at[pos], orecv.at[pos], o_s.at[pos], o_r.at[pos], qdev(pos)).wait_recv()
-        remote(tsend.at[pos], trecv.at[pos], st_s.at[pos], st_r.at[pos], qdev(pos)).wait_recv()
+        arrived(orecv.at[pos], o_r.at[pos])
+        arrived(trecv.at[pos], st_r.at[pos])
+        return [merge(a, b) for a, b in zip(state, part(pos))]
+
+    def take_loop(d, carry):
+        for m, (peak, total, o) in enumerate(take(d, [(ms[2 * m], ms[2 * m + 1], mo[m]) for m in range(2)])):
+            ms[2 * m] = peak
+            ms[2 * m + 1] = total
+            mo[m] = o
         return carry
 
-    lax.fori_loop(1, 8, o_wait, 0)
-
-    def merged(row, at):
-        peak = trecv[0, pl.ds(row, 1), :]
-        for n in range(1, R):
-            peak = jnp.maximum(peak, trecv[n, pl.ds(row, 1), :])
-        total = None
-        for n in range(R):
-            w = jnp.exp2(trecv[n, pl.ds(row, 1), :] - peak)
-            part = w * trecv[n, pl.ds(row + 1, 1), :]
-            o = w * orecv[n, pl.ds(at, VD), :].astype(F32)
-            total = (part, o) if total is None else (total[0] + part, total[1] + o)
-        return total[1] / total[0]
-
-    diff = merged(0, 0) - lam[0] * merged(2, VD)
+    for m, (peak, total, o) in enumerate(part(qpos)):
+        ms[2 * m] = peak
+        ms[2 * m + 1] = total
+        mo[m] = o
+    lax.fori_loop(0, 7, lambda i, carry: take_loop((4 + i + i // 4) % 8, carry), 0)
+    diff = mo[0] / ms[1] - lam[0] * (mo[1] / ms[3])
     diff = (diff * lax.rsqrt(jnp.mean(diff * diff, axis=0, keepdims=True) + EPS)).T
     g32 = gate[...].astype(F32)
     amix[...] = (diff * hgain[...] * (g32 / (1.0 + jnp.exp(-g32)))).astype(BF)
@@ -418,16 +439,19 @@
     for e in (4, 5, 3, 2, 6, 1, 7):
         a_copy((tp + e) % 8).start()
     arecv[:, mine] = amix[pl.ds(pl.multiple_of(tp * ROWS, ROWS), ROWS), :]
-    for e in (1, 7, 2, 6, 3, 5, 4):
-        src = (tp + e) % 8
-        arrived(arecv.at[:, pl.ds(pl.multiple_of(src * VD, VD), VD)], a_r.at[src])
-    for n in range(4):
-        cols = pl.ds(n * 512, 512)
-        out[:, cols] = (dot(arecv[...], wa[:, cols]) + csum[:, cols]).astype(BF)
+    def add_head(t):
+        cols = pl.ds(pl.multiple_of(t * VD, VD), VD)
+        csum[...] += dot(arecv[:, cols], wa[cols, :])
+
+    add_head(tp)
+    for t in (other, xl * 2 + c, xl * 2 + oc, xr * 2 + c, xr * 2 + oc, xo * 2 + c, xo * 2 + oc):
+        arrived(arecv.at[:, pl.ds(pl.multiple_of(t * VD, VD), VD)], a_r.at[t])
+        add_head(t)
+    out[...] = csum[...].astype(BF)
 
     for cp in pending:
         cp.wait_send()
-    for slot in range(6, 12):
+    for slot in (10, 11):
         wa_copy(tp, 0, slot, partner).wait_send()
     for d in range(1, 8):
         pos = (qpos + d) % 8
@@ -459,12 +483,13 @@
             v((R, 2 * VD, T), BF), v((R, 2 * VD, T), BF), v((R, 8, T), F32), v((R, 8, T), F32),
             v((2, T, VD), BF), v((2, VD, HALF), BF), v((4, 2 * ROWS, HALF), BF), v((8, ROWS, HALF), BF),
             v((8 * VD, D), BF), v((ROWS, D), F32), v((T, VD), BF), v((ROWS, 8 * VD), BF),
+            v((4, 1, T), F32), v((2, VD, T), F32),
             dma((12,)), dma((14,)), dma((8, 2)), dma((8,)), dma((8,)), dma((8,)), dma((8,)), dma((8,)), dma((9,)),
             dma((8,)), dma((8,)), dma((8,)), dma((8,)), dma((2,)), dma((2,)), dma, dma, dma, dma,
             dma((8,)), dma((8,)), dma((14,)), dma((8, 2)), dma((8,)), dma((8,)),
         ],
         compiler_params=pltpu.CompilerParams(
-            collective_id=0, has_side_effects=True, vmem_limit_bytes=67043328
+            collective_id=0, has_side_effects=True, vmem_limit_bytes=66500000
         ),
         name="layer",
     )(tokens, norm_gain.reshape(1, D), q1.T, k1.T, q2.T, k2.T, wv, wg, wo, wi, wx, taps, lam, hgain.reshape(1, VD), aw, cw)

time: 65 us -> 63.7 us (0.980)
  Pallas kernels: 62.6 us -> 61.2 us
    pallas_call x1, Pallas kernels: 62.6 us -> 61.2 us  [local(): pl.pallas_call(kernel, out_shape=jax.ShapeDtypeStruct((ROWS, D), BF), in_...]
where the time goes in v4:
time: 63.7 us; the launch traced here: 63.5 us
  Pallas kernels  61.2 us (96%)
  local copies, waits for them, and re-layouts  1.57 us (2%)
  between operations  0.66 us (1%)
    pallas_call x1, Pallas kernels, local(): pl.pallas_call(kernel, out_shape=jax.ShapeDtypeStruct((ROWS, D), BF), in_...  61.2 us
    unnamed x1, local copies, waits for them, and re-layouts  1.57 us

profile of v4, /device:TPU:1, one launch (start us, length us, event | category | flops | bytes accessed | tf_op | source)
XLA Modules:
  0.0 63.5 jit_solution(4235439604821264496)
XLA Ops:
  0.7 61.2 %layer.1 = bf16[32,2048]{1,0:T(8,128)(2,1)} custom-call(bf16[256,256]{1,0:T(8,128)(2,1)} %tok_h.1, f32[1,2048]{1,0:T(1,128)} %bitcast.10, bf16[64,2048]{1,0:T(8,128)(2,1)} %bitcast.6, bf16[64,2048]{1,0:T(8,128)(2,1)} %bitcast.7, bf16[64,2048]{1,0:T(8,128)(2,1)} %bitcast.8, bf16[64,2048]{1,0:T(8,128)(2,1)} %bitcast.9, bf16[2048,128]{1,0:T(8,128)(2,1)} %wv_h.1, ...), custom_call_target="tpu_custom_call" | custom-call | tf_op jit(solution)/shard_map/layer/pallas_call | solution.py:473
  61.9 1.6 %copy.19 = bf16[32,2048]{1,0:T(8,128)(2,1)} copy(bf16[32,2048]{1,0:T(8,128)(2,1)} %layer.1) | data formatting | bytes 262144

commit v5 on v4

--- a/solution.py
+++ b/solution.py
@@ -27,8 +27,8 @@
     tok_h, gain, wq1_h, wk1_h, wq2_h, wk2_h, wv_h, wg_h, wo_h, wi_h, wx_h, taps, lam, hgain, aw_h, cw_h,
     out,
     tok, wn, wall, acc, ss, kb, vb, qb, gate, outer, prod, edge, halo, s1, s2, osend, orecv, tsend, trecv,
-    mix, wout, psend, precv, wa, csum, amix, arecv, ms, mo,
-    lsem, tok_s, tok_r, k_s, k_r, v_s, v_r, q_s, q_r, o_s, o_r, st_s, st_r, h_s, h_r, m_s, m_r, w_s, w_r, p_s, p_r, wa_s, wa_r, a_s, a_r,
+    mix, wout, psend, precv, wa, csum, amix, arecv, ms, mo, rin, rstat,
+    lsem, tok_s, tok_r, k_s, k_r, v_s, v_r, q_s, q_r, o_s, o_r, st_s, st_r, h_s, h_r, m_s, m_r, w_s, w_r, p_s, p_r, wa_s, wa_r, a_s, a_r, x_s, x_r,
 ):
     sp = lax.axis_index("sp")
     tp = lax.axis_index("tp")
@@ -325,6 +325,55 @@
         o = dot(vb[n], p.astype(BF))
         return (part, o) if state is None else (state[0] + part, state[1] + o)
 
+    def merge(a, b):
+        peak = jnp.maximum(a[0], b[0])
+        wa_, wb_ = jnp.exp2(a[0] - peak), jnp.exp2(b[0] - peak)
+        return peak, wa_ * a[1] + wb_ * b[1], wa_ * a[2] + wb_ * b[2]
+
+    def o_copy(pos, m):
+        rows = pl.ds(m * VD, VD)
+        return remote(osend.at[pos, rows, :], orecv.at[qpos, rows, :], o_s.at[pos, m], o_r.at[qpos, m], qdev(pos))
+
+    def t_copy(pos):
+        return remote(tsend.at[pos], trecv.at[qpos], st_s.at[pos], st_r.at[qpos], qdev(pos))
+
+    def far_copies(m):
+        pos = (qpos + 4) % 8
+        dev = (q_right2, q_left2)[m]
+        return (
+            remote(osend.at[pos, pl.ds(m * VD, VD), :], rin.at[m], x_s.at[m], x_r.at[m], dev),
+            remote(tsend.at[pos], rstat.at[m], x_s.at[2 + m], x_r.at[2 + m], dev),
+        )
+
+    def send_far(m):
+        for cp in far_copies(m):
+            cp.start()
+
+    def send_part(i, pos, m):
+        @pl.when((i == 1) | (i == 2) | (i == 5) | (i == 6))
+        def _():
+            o_copy(pos, m).start()
+            if m == 1:
+                t_copy(pos).start()
+
+    def merge_far():
+        for m in range(2):
+            pos = (qpos + 2 + 4 * m) % 8
+            arrived(rin.at[m], x_r.at[m])
+            arrived(rstat.at[m], x_r.at[2 + m])
+            rows = pl.ds(m * VD, VD)
+            own, far = tsend[pos], rstat[m]
+            peak, total, o = merge(
+                (own[2 * m : 2 * m + 1], own[2 * m + 1 : 2 * m + 2], osend[pos, rows, :].astype(F32)),
+                (far[2 * m : 2 * m + 1], far[2 * m + 1 : 2 * m + 2], rin[m].astype(F32)),
+            )
+            osend[pos, rows, :] = o.astype(BF)
+            tsend[pos, pl.ds(2 * m, 1), :] = peak
+            tsend[pos, pl.ds(2 * m + 1, 1), :] = total
+            o_copy(pos, 0).start()
+            o_copy(pos, 1).start()
+            t_copy(pos).start()
+
     def ring_place(i):
         odd = i % 2
         mag = 4 - (i + 1) // 2
@@ -348,6 +397,7 @@
         peak2 = jnp.max(peak, axis=0, keepdims=True)
         sum1 = jnp.sum(state[0], axis=0, keepdims=True)
         osend[pos, pl.ds(0, VD), :] = state[1].astype(BF)
+        send_part(i, pos, 0)
         q1 = first_map(ring_place((i + 1) % 8))
         peak = None
         state = None
@@ -359,11 +409,14 @@
         osend[pos, pl.ds(VD, VD), :] = state[1].astype(BF)
         tsend[pos] = jnp.concatenate([peak1, sum1, peak2, sum2, peak1, sum1, peak2, sum2], axis=0)
 
-        @pl.when(i < 7)
+        send_part(i, pos, 1)
+
+        @pl.when(i == 0)
         def _():
-            remote(osend.at[pos], orecv.at[qpos], o_s.at[pos], o_r.at[qpos], qdev(pos)).start()
-            remote(tsend.at[pos], trecv.at[qpos], st_s.at[pos], st_r.at[qpos], qdev(pos)).start()
-
+            send_far(0)
+            send_far(1)
+
+        pl.when(i == 4)(merge_far)
         return next1
 
     q1 = first_map(ring_place(0))
@@ -375,6 +428,46 @@
     orecv[qpos] = osend[qpos]
     trecv[qpos] = tsend[qpos]
 
+    def part(n):
+        t = trecv[n]
+        return [
+            (t[2 * m : 2 * m + 1], t[2 * m + 1 : 2 * m + 2], orecv[n, pl.ds(m * VD, VD), :].astype(F32))
+            for m in range(2)
+        ]
+
+    def take(d, state):
+        pos = (qpos + d) % 8
+        for m in range(2):
+            arrived(orecv.at[pos, pl.ds(m * VD, VD), :], o_r.at[pos, m])
+        arrived(trecv.at[pos], st_r.at[pos])
+        return [merge(a, b) for a, b in zip(state, part(pos))]
+
+    def absorb(d):
+        for m, (peak, total, o) in enumerate(take(d, [(ms[2 * m], ms[2 * m + 1], mo[m]) for m in range(2)])):
+            ms[2 * m] = peak
+            ms[2 * m + 1] = total
+            mo[m] = o
+
+    for m, (peak, total, o) in enumerate(part(qpos)):
+        ms[2 * m] = peak
+        ms[2 * m + 1] = total
+        mo[m] = o
+    for d in (3, 5, 1, 7, 2, 6):
+        absorb(d)
+    diff = mo[0] / ms[1] - lam[0] * (mo[1] / ms[3])
+    diff = (diff * lax.rsqrt(jnp.mean(diff * diff, axis=0, keepdims=True) + EPS)).T
+    g32 = gate[...].astype(F32)
+    amix[...] = (diff * hgain[...] * (g32 / (1.0 + jnp.exp(-g32)))).astype(BF)
+
+    mine = pl.ds(pl.multiple_of(tp * VD, VD), VD)
+
+    def a_copy(t):
+        rows = pl.ds(pl.multiple_of(t * ROWS, ROWS), ROWS)
+        return remote(amix.at[rows, :], arecv.at[:, mine], a_s.at[t], a_r.at[tp], (sp, t))
+
+    for e in (4, 5, 3, 2, 6, 1, 7):
+        a_copy((tp + e) % 8).start()
+    arecv[:, mine] = amix[pl.ds(pl.multiple_of(tp * ROWS, ROWS), ROWS), :]
     wa_wait(xo * 2 + c, 0)
     wa_send(xo * 2 + c, 0, 12, partner)
     wa_wait(xo * 2 + c, 1)
@@ -395,50 +488,6 @@
         wa_wait(t, 0)
         wa_wait(t, 1)
 
-    def part(n):
-        t = trecv[n]
-        return [
-            (t[2 * m : 2 * m + 1], t[2 * m + 1 : 2 * m + 2], orecv[n, pl.ds(m * VD, VD), :].astype(F32))
-            for m in range(2)
-        ]
-
-    def merge(a, b):
-        peak = jnp.maximum(a[0], b[0])
-        wa_, wb_ = jnp.exp2(a[0] - peak), jnp.exp2(b[0] - peak)
-        return peak, wa_ * a[1] + wb_ * b[1], wa_ * a[2] + wb_ * b[2]
-
-    def take(d, state):
-        pos = (qpos + d) % 8
-        arrived(orecv.at[pos], o_r.at[pos])
-        arrived(trecv.at[pos], st_r.at[pos])
-        return [merge(a, b) for a, b in zip(state, part(pos))]
-
-    def take_loop(d, carry):
-        for m, (peak, total, o) in enumerate(take(d, [(ms[2 * m], ms[2 * m + 1], mo[m]) for m in range(2)])):
-            ms[2 * m] = peak
-            ms[2 * m + 1] = total
-            mo[m] = o
-        return carry
-
-    for m, (peak, total, o) in enumerate(part(qpos)):
-        ms[2 * m] = peak
-        ms[2 * m + 1] = total
-        mo[m] = o
-    lax.fori_loop(0, 7, lambda i, carry: take_loop((4 + i + i // 4) % 8, carry), 0)
-    diff = mo[0] / ms[1] - lam[0] * (mo[1] / ms[3])
-    diff = (diff * lax.rsqrt(jnp.mean(diff * diff, axis=0, keepdims=True) + EPS)).T
-    g32 = gate[...].astype(F32)
-    amix[...] = (diff * hgain[...] * (g32 / (1.0 + jnp.exp(-g32)))).astype(BF)
-
-    mine = pl.ds(pl.multiple_of(tp * VD, VD), VD)
-
-    def a_copy(t):
-        rows = pl.ds(pl.multiple_of(t * ROWS, ROWS), ROWS)
-        return remote(amix.at[rows, :], arecv.at[:, mine], a_s.at[t], a_r.at[tp], (sp, t))
-
-    for e in (4, 5, 3, 2, 6, 1, 7):
-        a_copy((tp + e) % 8).start()
-    arecv[:, mine] = amix[pl.ds(pl.multiple_of(tp * ROWS, ROWS), ROWS), :]
     def add_head(t):
         cols = pl.ds(pl.multiple_of(t * VD, VD), VD)
         csum[...] += dot(arecv[:, cols], wa[cols, :])
@@ -449,14 +498,16 @@
         add_head(t)
     out[...] = csum[...].astype(BF)
 
-    for cp in pending:
+    for cp in pending + [*far_copies(0), *far_copies(1)]:
         cp.wait_send()
     for slot in (10, 11):
         wa_copy(tp, 0, slot, partner).wait_send()
     for d in range(1, 8):
         pos = (qpos + d) % 8
-        remote(osend.at[pos], orecv.at[qpos], o_s.at[pos], o_r.at[qpos], qdev(pos)).wait_send()
-        remote(tsend.at[pos], trecv.at[qpos], st_s.at[pos], st_r.at[qpos], qdev(pos)).wait_send()
+        if d != 4:
+            o_copy(pos, 0).wait_send()
+            o_copy(pos, 1).wait_send()
+            t_copy(pos).wait_send()
         dst = (tp + d) % 8
         p_copy(dst // 2, dst % 2).wait_send()
         a_copy(dst).wait_send()
@@ -483,13 +534,13 @@
             v((R, 2 * VD, T), BF), v((R, 2 * VD, T), BF), v((R, 8, T), F32), v((R, 8, T), F32),
             v((2, T, VD), BF), v((2, VD, HALF), BF), v((4, 2 * ROWS, HALF), BF), v((8, ROWS, HALF), BF),
             v((8 * VD, D), BF), v((ROWS, D), F32), v((T, VD), BF), v((ROWS, 8 * VD), BF),
-            v((4, 1, T), F32), v((2, VD, T), F32),
+            v((4, 1, T), F32), v((2, VD, T), F32), v((2, VD, T), BF), v((2, 8, T), F32),
             dma((12,)), dma((14,)), dma((8, 2)), dma((8,)), dma((8,)), dma((8,)), dma((8,)), dma((8,)), dma((9,)),
-            dma((8,)), dma((8,)), dma((8,)), dma((8,)), dma((2,)), dma((2,)), dma, dma, dma, dma,
-            dma((8,)), dma((8,)), dma((14,)), dma((8, 2)), dma((8,)), dma((8,)),
+            dma((8, 2)), dma((8, 2)), dma((8,)), dma((8,)), dma((2,)), dma((2,)), dma, dma, dma, dma,
+            dma((8,)), dma((8,)), dma((14,)), dma((8, 2)), dma((8,)), dma((8,)), dma((4,)), dma((4,)),
         ],
         compiler_params=pltpu.CompilerParams(
-            collective_id=0, has_side_effects=True, vmem_limit_bytes=66500000
+            collective_id=0, has_side_effects=True, vmem_limit_bytes=56350000
         ),
         name="layer",
     )(tokens, norm_gain.reshape(1, D), q1.T, k1.T, q2.T, k2.T, wv, wg, wo, wi, wx, taps, lam, hgain.reshape(1, VD), aw, cw)

time: 63.7 us -> 61.3 us (0.962)
  Pallas kernels: 61.2 us -> 59.1 us
    pallas_call x1, Pallas kernels: 61.2 us -> 59.1 us  [local(): pl.pallas_call(kernel, out_shape=jax.ShapeDtypeStruct((ROWS, D), BF), in_...]
    unnamed x1 -> x7, local copies, waits for them, and re-layouts: 1.57 us -> 1.33 us
where the time goes in v5:
time: 61.3 us; the launch traced here: 61.1 us
  Pallas kernels  59.1 us (96%)
  local copies, waits for them, and re-layouts  1.33 us (2%)
  between operations  0.69 us (1%)
    pallas_call x1, Pallas kernels, local(): pl.pallas_call(kernel, out_shape=jax.ShapeDtypeStruct((ROWS, D), BF), in_...  59.1 us
    unnamed x7, local copies, waits for them, and re-layouts  1.33 us

profile of v5, /device:TPU:1, one launch (start us, length us, event | category | flops | bytes accessed | tf_op | source)
XLA Modules:
  0.0 61.1 jit_solution(4976514404297301828)
XLA Ops:
  0.0 0.0 copy-start
  0.7 0.0 copy-start.1
  0.7 0.0 copy-start.2
  0.7 0.0 copy-done
  0.7 0.7 %copy-done.1 = bf16[3,128]{1,0:T(4,128)(2,1)S(1)} copy-done((bf16[3,128]{1,0:T(4,128)(2,1)S(1)}, bf16[3,128]{1,0:T(4,128)(2,1)}, u32[]{:S(2)}) %copy-start.1) | copy-done | bytes 792
  1.3 0.0 copy-done.2
  1.4 59.1 %layer.1 = bf16[32,2048]{1,0:T(8,128)(2,1)S(1)} custom-call(bf16[256,256]{1,0:T(8,128)(2,1)} %tok_h.1, f32[1,2048]{1,0:T(1,128)S(1)} %bitcast.6, bf16[64,2048]{1,0:T(8,128)(2,1)} %bitcast.8, bf16[64,2048]{1,0:T(8,128)(2,1)} %bitcast.9, bf16[64,2048]{1,0:T(8,128)(2,1)} %bitcast.10, bf16[64,2048]{1,0:T(8,128)(2,1)} %bitcast.11, bf16[2048,128]{1,0:T(8,128)(2,1)} %wv_h.1, ...), custom_call_target="tpu_custom_call" | custom-call | tf_op jit(solution)/shard_map/layer/pallas_call | solution.py:524
  60.4 0.7 %copy.19 = bf16[32,2048]{1,0:T(8,128)(2,1)} copy(bf16[32,2048]{1,0:T(8,128)(2,1)S(1)} %layer.1) | data formatting | bytes 262144
Async XLA Ops:
  0.0 0.7 %copy-start = (f32[2048]{0:T(1024)S(1)}, f32[2048]{0:T(1024)}, u32[]{:S(2)}) copy-start(f32[2048]{0:T(1024)} %param.17) | copy-start | bytes 24580
  0.7 0.7 %copy-start.1 = (bf16[3,128]{1,0:T(4,128)(2,1)S(1)}, bf16[3,128]{1,0:T(4,128)(2,1)}, u32[]{:S(2)}) copy-start(bf16[3,128]{1,0:T(4,128)(2,1)} %taps.1) | copy-start | bytes 2308
  0.7 0.7 %copy-start.2 = (f32[128]{0:T(128)S(1)}, f32[128]{0:T(128)}, u32[]{:S(2)}) copy-start(f32[128]{0:T(128)} %param.29) | copy-start | bytes 1540

commit v6 on v5

--- a/solution.py
+++ b/solution.py
@@ -100,23 +100,25 @@
     def arrived(ref, rsem):
         remote(ref, ref, rsem, rsem, partner).wait_recv()
 
-    top, bottom = pl.ds(0, T // 2), pl.ds(T // 2, T // 2)
-    halves = (top, bottom)
-
-    def tok_send(t, half, slot, dev):
-        ref = tok.at[t, halves[half], :]
-        send(ref, ref, tok_s.at[slot], tok_r.at[t, half], dev)
-
-    def tok_wait(t, half):
-        arrived(tok.at[t, halves[half], :], tok_r.at[t, half])
+    def tok_part(t, part):
+        return tok.at[t, pl.ds(part * (T // 4), T // 4), :]
+
+    def tok_send(t, part, slot, dev):
+        send(tok_part(t, part), tok_part(t, part), tok_s.at[slot], tok_r.at[t, part], dev)
+
+    def tok_wait(t, part):
+        arrived(tok_part(t, part), tok_r.at[t, part])
+
+    def tok_block(t):
+        for part in range(4):
+            tok_wait(t, part)
 
     cp_tok.wait()
-    tok_send(tp, 0, 0, right_chip)
-    tok_send(tp, 1, 1, left_chip)
-    tok_send(tp, 1, 2, right_chip)
-    tok_send(tp, 0, 3, left_chip)
-    tok_send(tp, 0, 4, partner)
-    tok_send(tp, 1, 5, partner)
+    for part in range(4):
+        tok_send(tp, part, part, right_chip)
+        tok_send(tp, 3 - part, 4 + part, left_chip)
+    for part in range(4):
+        tok_send(tp, part, 8 + part, partner)
 
     for cp in loads[:9]:
         cp.wait()
@@ -141,34 +143,31 @@
     xl, xr, xo = (x + 3) % 4, (x + 1) % 4, (x + 2) % 4
     oc = 1 - c
     project(tp, True)
-    tok_wait(other, 0)
-    tok_wait(other, 1)
+    tok_block(other)
     project(other)
-    tok_wait(xl * 2 + c, 0)
-    tok_send(xl * 2 + c, 0, 6, right_chip)
-    tok_send(xl * 2 + c, 0, 7, partner)
-    tok_wait(xr * 2 + c, 1)
-    tok_send(xr * 2 + c, 1, 8, left_chip)
-    tok_send(xr * 2 + c, 1, 9, partner)
-    tok_wait(xl * 2 + c, 1)
-    tok_send(xl * 2 + c, 1, 10, partner)
-    tok_wait(xr * 2 + c, 0)
-    tok_send(xr * 2 + c, 0, 11, partner)
+    for n in range(2):
+        tok_wait(xl * 2 + c, n)
+        tok_send(xl * 2 + c, n, 12 + n, right_chip)
+        tok_wait(xr * 2 + c, 3 - n)
+        tok_send(xr * 2 + c, 3 - n, 14 + n, left_chip)
+        tok_send(xl * 2 + c, n, 16 + n, partner)
+        tok_send(xr * 2 + c, 3 - n, 18 + n, partner)
+    for n in range(2, 4):
+        tok_wait(xl * 2 + c, n)
+        tok_send(xl * 2 + c, n, 16 + n + 2, partner)
+        tok_wait(xr * 2 + c, 3 - n)
+        tok_send(xr * 2 + c, 3 - n, 18 + n + 2, partner)
     project(xl * 2 + c)
     project(xr * 2 + c)
-    tok_wait(xl * 2 + oc, 0)
-    tok_wait(xl * 2 + oc, 1)
+    tok_block(xl * 2 + oc)
     project(xl * 2 + oc)
-    tok_wait(xr * 2 + oc, 0)
-    tok_wait(xr * 2 + oc, 1)
+    tok_block(xr * 2 + oc)
     project(xr * 2 + oc)
-    tok_wait(xo * 2 + c, 0)
-    tok_send(xo * 2 + c, 0, 12, partner)
-    tok_wait(xo * 2 + c, 1)
-    tok_send(xo * 2 + c, 1, 13, partner)
+    for slot, part in enumerate((0, 3, 1, 2)):
+        tok_wait(xo * 2 + c, part)
+        tok_send(xo * 2 + c, part, 24 + slot, partner)
     project(xo * 2 + c)
-    tok_wait(xo * 2 + oc, 0)
-    tok_wait(xo * 2 + oc, 1)
+    tok_block(xo * 2 + oc)
     project(xo * 2 + oc)
 
     quarter = VD // 2
@@ -239,17 +238,17 @@
     k_send(at(kpos, 6), 5, k_right)
     arrived(kb.at[at(kpos, 2)], k_r.at[at(kpos, 2)])
     k_send(at(kpos, 2), 6, k_left)
-    arrived(vb.at[at(kpos, 2)], v_r.at[at(kpos, 2)])
-    v_send(at(kpos, 2), 4, k_left2)
-    v_send(at(kpos, 2), 5, k_left)
-    arrived(vb.at[at(kpos, 6)], v_r.at[at(kpos, 6)])
-    v_send(at(kpos, 6), 6, k_right)
     arrived(qb.at[at(qpos, 6)], q_r.at[at(qpos, 6)])
     q_part(at(qpos, 6), 0, 4, q_right2)
     q_send(at(qpos, 6), 5, q_right)
     arrived(qb.at[at(qpos, 2)], q_r.at[at(qpos, 2)])
     q_part(at(qpos, 2), 1, 6, q_left2)
     q_send(at(qpos, 2), 7, q_left)
+    arrived(vb.at[at(kpos, 2)], v_r.at[at(kpos, 2)])
+    v_send(at(kpos, 2), 4, k_left2)
+    v_send(at(kpos, 2), 5, k_left)
+    arrived(vb.at[at(kpos, 6)], v_r.at[at(kpos, 6)])
+    v_send(at(kpos, 6), 6, k_right)
     to_prev.wait_recv()
     to_next.wait_recv()
     before = jnp.where(sp == 0, 0.0, halo[0][7:8, :])
@@ -535,7 +534,7 @@
             v((2, T, VD), BF), v((2, VD, HALF), BF), v((4, 2 * ROWS, HALF), BF), v((8, ROWS, HALF), BF),
             v((8 * VD, D), BF), v((ROWS, D), F32), v((T, VD), BF), v((ROWS, 8 * VD), BF),
             v((4, 1, T), F32), v((2, VD, T), F32), v((2, VD, T), BF), v((2, 8, T), F32),
-            dma((12,)), dma((14,)), dma((8, 2)), dma((8,)), dma((8,)), dma((8,)), dma((8,)), dma((8,)), dma((9,)),
+            dma((12,)), dma((28,)), dma((8, 4)), dma((8,)), dma((8,)), dma((8,)), dma((8,)), dma((8,)), dma((9,)),
             dma((8, 2)), dma((8, 2)), dma((8,)), dma((8,)), dma((2,)), dma((2,)), dma, dma, dma, dma,
             dma((8,)), dma((8,)), dma((14,)), dma((8, 2)), dma((8,)), dma((8,)), dma((4,)), dma((4,)),
         ],

time: 61.3 us -> 60.8 us (level)
  no operation moved by 1% of the time
where the time goes in v6:
time: 60.8 us; the launch traced here: 60.6 us
  Pallas kernels  58.6 us (96%)
  local copies, waits for them, and re-layouts  1.33 us (2%)
  between operations  0.69 us (1%)
    pallas_call x1, Pallas kernels, local(): pl.pallas_call(kernel, out_shape=jax.ShapeDtypeStruct((ROWS, D), BF), in_...  58.6 us
    unnamed x7, local copies, waits for them, and re-layouts  1.33 us

profile of v6, /device:TPU:1, one launch (start us, length us, event | category | flops | bytes accessed | tf_op | source)
XLA Modules:
  0.0 60.6 jit_solution(9682103911668383155)
XLA Ops:
  0.0 0.0 copy-start
  0.7 0.0 copy-start.1
  0.7 0.0 copy-start.2
  0.7 0.0 copy-done
  0.7 0.7 %copy-done.1 = bf16[3,128]{1,0:T(4,128)(2,1)S(1)} copy-done((bf16[3,128]{1,0:T(4,128)(2,1)S(1)}, bf16[3,128]{1,0:T(4,128)(2,1)}, u32[]{:S(2)}) %copy-start.1) | copy-done | bytes 792
  1.3 0.0 copy-done.2
  1.4 58.6 %layer.1 = bf16[32,2048]{1,0:T(8,128)(2,1)S(1)} custom-call(bf16[256,256]{1,0:T(8,128)(2,1)} %tok_h.1, f32[1,2048]{1,0:T(1,128)S(1)} %bitcast.6, bf16[64,2048]{1,0:T(8,128)(2,1)} %bitcast.8, bf16[64,2048]{1,0:T(8,128)(2,1)} %bitcast.9, bf16[64,2048]{1,0:T(8,128)(2,1)} %bitcast.10, bf16[64,2048]{1,0:T(8,128)(2,1)} %bitcast.11, bf16[2048,128]{1,0:T(8,128)(2,1)} %wv_h.1, ...), custom_call_target="tpu_custom_call" | custom-call | tf_op jit(solution)/shard_map/layer/pallas_call | solution.py:523
  60.0 0.7 %copy.19 = bf16[32,2048]{1,0:T(8,128)(2,1)} copy(bf16[32,2048]{1,0:T(8,128)(2,1)S(1)} %layer.1) | data formatting | bytes 262144
Async XLA Ops:
  0.0 0.7 %copy-start = (f32[2048]{0:T(1024)S(1)}, f32[2048]{0:T(1024)}, u32[]{:S(2)}) copy-start(f32[2048]{0:T(1024)} %param.17) | copy-start | bytes 24580
  0.7 0.7 %copy-start.1 = (bf16[3,128]{1,0:T(4,128)(2,1)S(1)}, bf16[3,128]{1,0:T(4,128)(2,1)}, u32[]{:S(2)}) copy-start(bf16[3,128]{1,0:T(4,128)(2,1)} %taps.1) | copy-start | bytes 2308
  0.7 0.7 %copy-start.2 = (f32[128]{0:T(128)S(1)}, f32[128]{0:T(128)}, u32[]{:S(2)}) copy-start(f32[128]{0:T(128)} %param.29) | copy-start | bytes 1540

commit v7 on v6

--- a/solution.py
+++ b/solution.py
@@ -384,7 +384,7 @@
     def second_map(pos):
         return jnp.concatenate([zero, qb[pos, pl.ds(KD, KD), :]], axis=0)
 
-    def one_block(i, peak1):
+    def one_block(i, peak1, last=False):
         pos = ring_place(i)
         pl.when(i == 2)(wa_forward)
         q2 = second_map(pos)
@@ -397,13 +397,14 @@
         sum1 = jnp.sum(state[0], axis=0, keepdims=True)
         osend[pos, pl.ds(0, VD), :] = state[1].astype(BF)
         send_part(i, pos, 0)
-        q1 = first_map(ring_place((i + 1) % 8))
+        q1 = None if last else first_map(ring_place((i + 1) % 8))
         peak = None
         state = None
         for n in range(R):
-            peak = scores(q1, n, s1, peak)
+            if not last:
+                peak = scores(q1, n, s1, peak)
             state = apply(n, s2, peak2, state)
-        next1 = jnp.max(peak, axis=0, keepdims=True)
+        next1 = peak1 if last else jnp.max(peak, axis=0, keepdims=True)
         sum2 = jnp.sum(state[0], axis=0, keepdims=True)
         osend[pos, pl.ds(VD, VD), :] = state[1].astype(BF)
         tsend[pos] = jnp.concatenate([peak1, sum1, peak2, sum2, peak1, sum1, peak2, sum2], axis=0)
@@ -422,7 +423,8 @@
     peak = None
     for n in range(R):
         peak = scores(q1, n, s1, peak)
-    lax.fori_loop(0, 8, one_block, jnp.max(peak, axis=0, keepdims=True))
+    peak = lax.fori_loop(0, 7, one_block, jnp.max(peak, axis=0, keepdims=True))
+    one_block(7, peak, last=True)
 
     orecv[qpos] = osend[qpos]
     trecv[qpos] = tsend[qpos]

time: 60.8 us -> 61.1 us (level)
  no operation moved by 1% of the time
where the time goes in v7:
time: 61.1 us; the launch traced here: 60.9 us
  Pallas kernels  58.9 us (96%)
  local copies, waits for them, and re-layouts  1.33 us (2%)
  between operations  0.69 us (1%)
    pallas_call x1, Pallas kernels, local(): pl.pallas_call(kernel, out_shape=jax.ShapeDtypeStruct((ROWS, D), BF), in_...  58.9 us
    unnamed x7, local copies, waits for them, and re-layouts  1.33 us

profile of v7, /device:TPU:1, one launch (start us, length us, event | category | flops | bytes accessed | tf_op | source)
XLA Modules:
  0.0 60.9 jit_solution(5596270647549600557)
XLA Ops:
  0.0 0.0 copy-start
  0.7 0.0 copy-start.1
  0.7 0.0 copy-start.2
  0.7 0.0 copy-done
  0.7 0.7 %copy-done.1 = bf16[3,128]{1,0:T(4,128)(2,1)S(1)} copy-done((bf16[3,128]{1,0:T(4,128)(2,1)S(1)}, bf16[3,128]{1,0:T(4,128)(2,1)}, u32[]{:S(2)}) %copy-start.1) | copy-done | bytes 792
  1.3 0.0 copy-done.2
  1.4 58.9 %layer.1 = bf16[32,2048]{1,0:T(8,128)(2,1)S(1)} custom-call(bf16[256,256]{1,0:T(8,128)(2,1)} %tok_h.1, f32[1,2048]{1,0:T(1,128)S(1)} %bitcast.6, bf16[64,2048]{1,0:T(8,128)(2,1)} %bitcast.8, bf16[64,2048]{1,0:T(8,128)(2,1)} %bitcast.9, bf16[64,2048]{1,0:T(8,128)(2,1)} %bitcast.10, bf16[64,2048]{1,0:T(8,128)(2,1)} %bitcast.11, bf16[2048,128]{1,0:T(8,128)(2,1)} %wv_h.1, ...), custom_call_target="tpu_custom_call" | custom-call | tf_op jit(solution)/shard_map/layer/pallas_call | solution.py:525
  60.3 0.7 %copy.19 = bf16[32,2048]{1,0:T(8,128)(2,1)} copy(bf16[32,2048]{1,0:T(8,128)(2,1)S(1)} %layer.1) | data formatting | bytes 262144
Async XLA Ops:
  0.0 0.7 %copy-start = (f32[2048]{0:T(1024)S(1)}, f32[2048]{0:T(1024)}, u32[]{:S(2)}) copy-start(f32[2048]{0:T(1024)} %param.17) | copy-start | bytes 24580
  0.7 0.7 %copy-start.1 = (bf16[3,128]{1,0:T(4,128)(2,1)S(1)}, bf16[3,128]{1,0:T(4,128)(2,1)}, u32[]{:S(2)}) copy-start(bf16[3,128]{1,0:T(4,128)(2,1)} %taps.1) | copy-start | bytes 2308
  0.7 0.7 %copy-start.2 = (f32[128]{0:T(128)S(1)}, f32[128]{0:T(128)}, u32[]{:S(2)}) copy-start(f32[128]{0:T(128)} %param.29) | copy-start | bytes 1540
